TPU v7x, 32 devices: a whole 2x2x4 slice. The times are simulated.
32 devices in a mesh: sp: 16 (over z, y, x), tp: 2 (over core).
Axes of the slice: x: 2, y: 2, z: 4, core: 2. Of those that a mesh axis runs over, the one named last changes fastest.
Arguments:
- tokens: bfloat16 [2048, 2048], P('sp'), may hold values from -6 to 6
- in_gain: bfloat16 [2048], replicated, may hold values from 0.099609375 to 1.8984375
- w_value: bfloat16 [2048, 4096], P('sp', 'tp'), may hold values from -0.125 to 0.125
- w_gate: bfloat16 [2048, 4096], P('sp', 'tp'), may hold values from -0.125 to 0.125
- w_in_key: bfloat16 [2048, 1024], P('sp', 'tp'), may hold values from -0.125 to 0.125
- w_read: bfloat16 [2048, 1024], P('sp', 'tp'), may hold values from -0.125 to 0.125
- w_step_fwd: bfloat16 [2048, 64], P('sp', 'tp'), may hold values from -0.25 to 0.25
- w_step_bwd: bfloat16 [2048, 64], P('sp', 'tp'), may hold values from -0.25 to 0.25
- conv_value: bfloat16 [5, 4096], P(None, 'tp'), may hold values from -2.5 to 2.5
- conv_key: bfloat16 [5, 1024], P(None, 'tp'), may hold values from -2.5 to 2.5
- conv_read: bfloat16 [5, 1024], P(None, 'tp'), may hold values from -2.5 to 2.5
- step_bias: float32 [2, 64], P(None, 'tp'), may hold values from -4 to -2
- rate: float32 [2, 64], P(None, 'tp'), may hold values from 0 to 1, as said below
- norm_gain: bfloat16 [4096], P('tp'), may hold values from 0.099609375 to 1.8984375
- w_out: bfloat16 [4096, 2048], P('tp', 'sp'), may hold values from -0.09375 to 0.09375
Outputs:
- mixed: bfloat16 [2048, 2048], P('sp')
Inputs may be any that keep to these rules, and one draw needn't show every extreme that they name: `rate`: positive decay rates, one per head and direction.
All inputs are finite; a program needn't handle non-finite values.
Results may differ from a plain program's by a relative error of at most 0.018.
Values may be sent and summed in bfloat16 or wider, within the bound.
A program may use at most 128 MiB of HBM per device.

v0:
```python
import jax
import jax.numpy as jnp
from jax import lax
from jax.sharding import PartitionSpec as P

HEAD_DIM = 64
STATE = 128
KERNEL = 5
BLOCK = 128


EPSILON = 1e-05
FULL_PRECISION = lax.Precision.HIGHEST


def entering_2(x, axis, combine, identity, reverse):
    length, place = (lax.axis_size(axis), lax.axis_index(axis))
    everything = jax.tree.map(lambda part: lax.all_gather(part, axis), x)
    start = jax.tree.map(
        lambda part, zero: jnp.broadcast_to(jnp.asarray(zero, part.dtype), part.shape), x, identity
    )

    def step(k, before):
        at = length - 1 - k if reverse else k
        reached = at > place if reverse else at < place
        new = combine(before, jax.tree.map(lambda part: part[at], everything))
        return jax.tree.map(lambda a, b: jnp.where(reached, a, b), new, before)

    return lax.fori_loop(0, length, step, start)


def with_halo(cells, sides, width):
    for axis, dim in sides:
        count = lax.axis_size(axis)
        ends = count - 1
        head = lax.slice_in_dim(cells, 0, width, axis=dim)
        tail = lax.slice_in_dim(cells, cells.shape[dim] - width, cells.shape[dim], axis=dim)
        cells = jnp.concatenate(
            [
                lax.ppermute(tail, axis, [(i, (i + 1) % count) for i in range(ends)]),
                cells,
                lax.ppermute(head, axis, [((i + 1) % count, i) for i in range(ends)]),
            ],
            axis=dim,
        )
    return cells


def normalize(tensor, gain):
    return tensor * lax.rsqrt(jnp.mean(tensor * tensor, -1, keepdims=True) + EPSILON) * gain


def block_parts(values, step_size, log_decay, in_keys):
    per_group = values.shape[1] // in_keys.shape[1]
    cumulative = jnp.cumsum(log_decay, axis=0)
    log_total = cumulative[-1]
    weighting = jnp.exp(log_total[None, :] - cumulative) * step_size
    key_heads = jnp.repeat(in_keys, per_group, axis=1)
    scaled = (values.astype(jnp.float32) * weighting[:, :, None]).astype(jnp.bfloat16)
    injected = jnp.einsum("jhn,jhp->hpn", key_heads, scaled, preferred_element_type=jnp.float32)
    return (cumulative, jnp.exp(log_total), injected)


def block_step(memory, inputs):
    values, step_size, cumulative, damping, injected, in_keys, read_in = inputs
    per_group = values.shape[1] // in_keys.shape[1]
    scores = jnp.einsum("ign,jgn->ijg", read_in, in_keys, preferred_element_type=jnp.float32)
    scores = jnp.repeat(scores, per_group, axis=2)
    length = values.shape[0]
    below_mask = (jnp.arange(length)[:, None] >= jnp.arange(length)[None, :])[:, :, None]
    gaps = jnp.where(below_mask, cumulative[:, None, :] - cumulative[None, :, :], -jnp.inf)
    weights = (scores * jnp.exp(gaps) * step_size[None, :, :]).astype(jnp.bfloat16)
    within = jnp.einsum("ijh,jhp->ihp", weights, values, preferred_element_type=jnp.float32)
    read_heads = jnp.repeat(read_in.astype(jnp.float32), per_group, axis=1)
    carried = (
        jnp.einsum("ihn,hpn->ihp", read_heads, memory, precision=FULL_PRECISION)
        * jnp.exp(cumulative)[:, :, None]
    )
    memory = damping[:, None, None] * memory + injected
    return (memory, within + carried)


def blocked(tensor):
    blocks = tensor.shape[0] // BLOCK
    return tensor.reshape((blocks, BLOCK) + tensor.shape[1:])


def sweep(block_inputs, memory):
    memory, swept = lax.scan(block_step, memory, block_inputs)
    return (swept.reshape((swept.shape[0] * swept.shape[1],) + swept.shape[2:]), memory)


def settle(damping_blocks, injected_blocks, memory):

    def advance(memory, inputs):
        return (inputs[0][:, None, None] * memory + inputs[1], None)

    memory, unused = lax.scan(advance, memory, (damping_blocks, injected_blocks))
    return memory


def chain(before_pair, after_pair):
    return (
        before_pair[0] * after_pair[0],
        after_pair[0][:, None, None] * before_pair[1] + after_pair[1],
    )


def entering(damping, final_state, backward):
    identity_pair = (jnp.ones_like(damping), jnp.zeros_like(final_state))
    if backward:
        arrived = entering_2((damping, final_state), "sp", chain, identity_pair, True)
    else:
        arrived = entering_2((damping, final_state), "sp", chain, identity_pair, False)
    return arrived[1]


def body(
    tokens,
    in_gain,
    w_value,
    w_gate,
    w_in_key,
    w_read,
    w_step_fwd,
    w_step_bwd,
    conv_value,
    conv_key,
    conv_read,
    step_bias,
    rate,
    norm_gain,
    w_out,
):
    normed = normalize(tokens.astype(jnp.float32), in_gain.astype(jnp.float32)).astype(jnp.bfloat16)
    weights = (
        lax.all_gather(w_value, "sp", axis=0, tiled=True),
        lax.all_gather(w_gate, "sp", axis=0, tiled=True),
        lax.all_gather(w_in_key, "sp", axis=0, tiled=True),
        lax.all_gather(w_read, "sp", axis=0, tiled=True),
        lax.all_gather(w_step_fwd, "sp", axis=0, tiled=True),
        lax.all_gather(w_step_bwd, "sp", axis=0, tiled=True),
    )
    projected = [
        jnp.dot(normed, weight, preferred_element_type=jnp.float32).astype(jnp.bfloat16)
        for weight in weights
    ]
    value_raw, gate_raw, key_raw, read_raw, pre_fwd, pre_bwd = projected
    value_cols = value_raw.shape[1]
    key_cols = key_raw.shape[1]
    joined = jnp.concatenate([value_raw, key_raw, read_raw], axis=1)
    padded = with_halo(joined, (("sp", 0),), (KERNEL - 1) // 2)
    kernel_taps = jnp.concatenate([conv_value, conv_key, conv_read], axis=1).astype(jnp.float32)
    length = joined.shape[0]
    summed = jnp.zeros(joined.shape, jnp.float32)
    for offset in range(KERNEL):
        summed = summed + padded[offset : offset + length].astype(jnp.float32) * kernel_taps[offset]
    mixed_in = jax.nn.silu(summed).astype(jnp.bfloat16)
    head_count = value_cols // HEAD_DIM
    group_count = key_cols // STATE
    values = mixed_in[:, :value_cols].reshape(length, head_count, HEAD_DIM)
    in_keys = mixed_in[:, value_cols : value_cols + key_cols].reshape(length, group_count, STATE)
    read_in = mixed_in[:, value_cols + key_cols :].reshape(length, group_count, STATE)
    blank = jnp.zeros((head_count, HEAD_DIM, STATE), jnp.float32)
    summed_heads = jnp.zeros(values.shape, jnp.float32)
    for direction, step_pre in ((0, pre_fwd), (1, pre_bwd)):
        step_size = jax.nn.softplus(step_pre.astype(jnp.float32) + step_bias[direction])
        log_decay = -rate[direction] * step_size
        ordered = (values, step_size, log_decay, in_keys, read_in)
        if direction == 1:
            ordered = tuple((tensor[::-1] for tensor in ordered))
        value_blocks, step_blocks, decay_blocks, key_blocks, read_blocks = [
            blocked(tensor) for tensor in ordered
        ]
        cumulative_blocks, damping_blocks, injected_blocks = jax.vmap(block_parts)(
            value_blocks, step_blocks, decay_blocks, key_blocks
        )
        block_inputs = (
            value_blocks,
            step_blocks,
            cumulative_blocks,
            damping_blocks,
            injected_blocks,
            key_blocks,
            read_blocks,
        )
        damping = jnp.exp(jnp.sum(ordered[2], axis=0))
        final_state = settle(damping_blocks, injected_blocks, blank)
        arriving = entering(damping, final_state, direction == 1)
        swept, final_state = sweep(block_inputs, arriving)
        if direction == 1:
            swept = swept[::-1]
        summed_heads = summed_heads + swept
    gated_out = summed_heads * jax.nn.silu(gate_raw.astype(jnp.float32)).reshape(values.shape)
    head_gain = norm_gain.astype(jnp.float32).reshape(head_count, HEAD_DIM)
    normed_heads = normalize(gated_out, head_gain).astype(jnp.bfloat16).reshape(length, value_cols)
    out_whole = lax.all_gather(w_out, "sp", axis=1, tiled=True)
    own_rows = lax.psum_scatter(
        jnp.dot(normed_heads, out_whole, preferred_element_type=jnp.float32).astype(jnp.bfloat16),
        "tp",
        scatter_dimension=0,
        tiled=True,
    )
    return lax.all_gather(own_rows, "tp", axis=0, tiled=True)


def solution(mesh):
    in_specs = (
        P("sp", None),
        P(),
        P("sp", "tp"),
        P("sp", "tp"),
        P("sp", "tp"),
        P("sp", "tp"),
        P("sp", "tp"),
        P("sp", "tp"),
        P(None, "tp"),
        P(None, "tp"),
        P(None, "tp"),
        P(None, "tp"),
        P(None, "tp"),
        P("tp"),
        P("tp", "sp"),
    )
    out_specs = P("sp", None)
    return jax.shard_map(body, mesh=mesh, in_specs=in_specs, out_specs=out_specs, check_vma=False)
```

profile of v0, /device:TPU:19, one launch (start us, length us, event | category | flops | bytes accessed | tf_op | source)
XLA Modules:
  0.0 912.6 jit_solution(5155035797716013802)
XLA Ops:
  10.1 23.0 %all_gather.46 = bf16[2048,32]{0,1:T(8,128)(2,1)S(1)} all-gather(bf16[128,32]{0,1:T(8,128)(2,1)} %param.26), channel_id=1, replica_groups=mesh['sp'=16,'tp'=2] {'sp'}, dimensions={0}, use_global_device_ids=true | all-gather | bytes 139264 | tf_op jit(solution)/shard_map/all_gather | solution.py:142
  37.7 32.4 %all-gather.16.cloned.1.call-done = bf16[2048,512]{1,0:T(8,128)(2,1)} async-done(((bf16[128,512]{1,0:T(8,128)(2,1)}), bf16[2048,512]{1,0:T(8,128)(2,1)}) %all-gather.16.cloned.1.call-update) | async-done | bytes 2097168 | tf_op jit(solution)/shard_map/all_gather | solution.py:140
  70.2 2.1 convolution_convert_fusion.3
  72.2 59.9 %all-gather.14.cloned.1.call-done = bf16[2048,512]{1,0:T(8,128)(2,1)} async-done(((bf16[128,512]{1,0:T(8,128)(2,1)}), bf16[2048,512]{1,0:T(8,128)(2,1)}) %all-gather.14.cloned.1.call-update) | async-done | bytes 2097168 | tf_op jit(solution)/shard_map/all_gather | solution.py:139
  132.1 2.1 convolution_convert_fusion.4
  134.2 111.4 %all-gather.12.cloned.1.call-done = bf16[2048,2048]{1,0:T(8,128)(2,1)} async-done(((bf16[128,2048]{1,0:T(8,128)(2,1)}), bf16[2048,2048]{1,0:T(8,128)(2,1)}) %all-gather.12.cloned.1.call-update) | async-done | bytes 8388624 | tf_op jit(solution)/shard_map/all_gather | solution.py:137
  245.6 4.7 convolution_convert_fusion.2
  250.4 3.3 collective-permute-start
  255.7 3.3 collective-permute-done.1
  264.6 24.5 %all_gather.43 = bf16[2048,32]{0,1:T(8,128)(2,1)S(1)} all-gather(bf16[128,32]{0,1:T(8,128)(2,1)S(1)} %copy-done.19), channel_id=1, replica_groups=mesh['sp'=16,'tp'=2] {'sp'}, dimensions={0}, use_global_device_ids=true | all-gather | bytes 139264 | tf_op jit(solution)/shard_map/all_gather | solution.py:141
  294.8 31.4 %all-reduce.2 = (f32[512]{0:T(512)S(1)}, f32[512]{0:T(512)S(1)}) all-reduce(f32[512]{0:T(512)S(1)} %exponential_dynamic-update-slice_fusion, f32[512]{0:T(512)S(1)} %exponential_dynamic-update-slice_fusion.1), channel_id=4, replica_groups=mesh['sp'=16,'tp'=2] {'sp'}, use_global_device_ids=true, to_apply=%add.1 | all-reduce | flops 1024 | bytes 8192
  328.7 32.5 %all-gather.18.cloned.1.call-done = bf16[2048,2048]{1,0:T(8,128)(2,1)} async-done(((bf16[128,2048]{1,0:T(8,128)(2,1)}), bf16[2048,2048]{1,0:T(8,128)(2,1)}) %all-gather.18.cloned.1.call-update) | async-done | bytes 8388624 | tf_op jit(solution)/shard_map/all_gather | solution.py:138
  361.2 4.9 divide_multiply_fusion
  377.1 3.0 fusion.6
  383.7 170.0 %all-gather.24.cloned.1.call-done = f32[512,64,128]{2,1,0:T(8,128)} async-done(((f32[32,64,128]{2,1,0:T(8,128)}), f32[512,64,128]{2,1,0:T(8,128)}) %all-gather.24.cloned.1.call-update) | async-done | bytes 16777232 | tf_op jit(solution)/shard_map/all_gather | solution.py:18
  553.8 34.8 %while.21 = (s32[]{:T(128)}, f32[32,64,128]{2,1,0:T(8,128)S(1)}, s32[]{:T(128)}, f32[16,32]{1,0:T(8,128)}, f32[16,32,64,128]{3,2,1,0:T(8,128)}, /*index=5*/s32[]{:T(128)}, s32[]{:T(128)}, s32[]{:T(128)}, s32[]{:T(128)}) while((s32[]{:T(128)}, f32[32,64,128]{2,1,0:T(8,128)S(1)}, s32[]{:T(128)}, f32[16,32]{1,0:T(8,128)}, ...), condition=%wide.region_8.9_spmd.clone, body=%wide.region_7.8_spmd.clone.sunk | while | flops 1048584 | bytes 3146279 | solution.py:29
  589.8 5.1 fusion.11
  596.4 149.2 %all-gather.22.cloned.1.call-done = f32[512,64,128]{2,1,0:T(8,128)} async-done(((f32[32,64,128]{2,1,0:T(8,128)}), f32[512,64,128]{2,1,0:T(8,128)}) %all-gather.22.cloned.1.call-update) | async-done | bytes 16777232 | tf_op jit(solution)/shard_map/all_gather | solution.py:18
  745.6 34.7 %while.20 = (s32[]{:T(128)}, f32[32,64,128]{2,1,0:T(8,128)S(1)}, s32[]{:T(128)}, f32[16,32]{1,0:T(8,128)}, f32[16,32,64,128]{3,2,1,0:T(8,128)}, /*index=5*/s32[]{:T(128)}, s32[]{:T(128)}) while((s32[]{:T(128)}, f32[32,64,128]{2,1,0:T(8,128)S(1)}, s32[]{:T(128)}, f32[16,32]{1,0:T(8,128)}, f32[16,32,64,128]{3,2,1,0:T(8,128)}, ...), condition=%wide.region_4.5_spmd.clone, body=%wide.region_3.4_spmd.clone.sunk | while | flops 1048580 | bytes 3146217 | solution.py:29
  781.9 5.2 multiply_reduce_fusion
  789.1 98.4 %all-gather.20.cloned.1.call-done = bf16[2048,2048]{1,0:T(8,128)(2,1)} async-done(((bf16[2048,128]{1,0:T(8,128)(2,1)}), bf16[2048,2048]{1,0:T(8,128)(2,1)}) %all-gather.20.cloned.1.call-update) | async-done | bytes 8388624 | tf_op jit(solution)/shard_map/all_gather | solution.py:197
  887.5 5.5 convolution_convert_fusion
  893.0 9.5 %reduce-scatter.2.cloned.1.call-done = bf16[64,2048]{1,0:T(8,128)(2,1)} async-done(((bf16[128,2048]{1,0:T(8,128)(2,1)}), bf16[64,2048]{1,0:T(8,128)(2,1)}) %reduce-scatter.2.cloned.1.call-update) | async-done | bytes 262160 | tf_op jit(solution)/shard_map/reduce_scatter | solution.py:198
  902.6 2.4 all_gather.51
  (196 shorter events, 113.4 us)
Async XLA Ops:
  6.5 63.6 %copy-start.7 = (bf16[128,2048]{1,0:T(8,128)(2,1)S(1)}, bf16[128,2048]{1,0:T(8,128)(2,1)}, u32[]{:S(2)}) copy-start(bf16[128,2048]{1,0:T(8,128)(2,1)} %param.19) | copy-start | bytes 1572868
  6.5 31.1 %copy-start.16 = (bf16[5,2048]{1,0:T(8,128)(2,1)S(1)}, bf16[5,2048]{1,0:T(8,128)(2,1)}, u32[]{:S(2)}) copy-start(bf16[5,2048]{1,0:T(8,128)(2,1)} %param.27) | copy-start | bytes 61444
  6.5 31.1 %copy-start.18 = (bf16[5,512]{1,0:T(8,128)(2,1)S(1)}, bf16[5,512]{1,0:T(8,128)(2,1)}, u32[]{:S(2)}) copy-start(bf16[5,512]{1,0:T(8,128)(2,1)} %param.28) | copy-start | bytes 15364
  6.5 31.1 %copy-start.17 = (bf16[5,512]{1,0:T(8,128)(2,1)S(1)}, bf16[5,512]{1,0:T(8,128)(2,1)}, u32[]{:S(2)}) copy-start(bf16[5,512]{1,0:T(8,128)(2,1)} %param.29) | copy-start | bytes 15364
  6.5 63.6 %all-gather.16.cloned.1.call-start = ((), (), s32[]{:S(2)}) async-start(), calls=%async_computation.3 | async-start | bytes 2228224 | tf_op jit(solution)/shard_map/all_gather | solution.py:140
  7.3 124.9 %all-gather.14.cloned.1.call-start = ((), (), s32[]{:S(2)}) async-start(), calls=%async_computation.2 | async-start | bytes 2228224 | tf_op jit(solution)/shard_map/all_gather | solution.py:139
  8.0 237.6 %all-gather.12.cloned.1.call-start = ((), (), s32[]{:S(2)}) async-start(), calls=%async_computation.1 | async-start | bytes 8912896 | tf_op jit(solution)/shard_map/all_gather | solution.py:137
  8.8 352.4 %all-gather.18.cloned.1.call-start = ((), (), s32[]{:S(2)}) async-start(), calls=%async_computation.4 | async-start | bytes 8912896 | tf_op jit(solution)/shard_map/all_gather | solution.py:138
  9.3 544.4 %all-gather.24.cloned.1.call-start = ((), (), s32[]{:S(2)}) async-start(), calls=%async_computation.8 | async-start | bytes 17825792 | tf_op jit(solution)/shard_map/all_gather | solution.py:18
  34.3 254.8 %copy-start.21 = (f32[128]{0:T(128)}, f32[128]{0:T(128)S(1)}, u32[]{:S(2)}) copy-start(f32[128]{0:T(128)S(1)} %add_rsqrt_fusion.1) | copy-start | bytes 1540
  250.4 5.3 collective-permute-start
  253.7 5.3 collective-permute-start.1
  260.8 30.1 %copy-start = (bf16[128,2048]{0,1:T(8,128)(2,1)}, bf16[128,2048]{0,1:T(8,128)(2,1)S(1)}, u32[]{:S(2)}) copy-start(bf16[128,2048]{0,1:T(8,128)(2,1)S(1)} %copy.49) | copy-start | bytes 1572868
  264.5 481.1 %all-gather.22.cloned.1.call-start = ((), (), s32[]{:S(2)}) async-start(), calls=%async_computation.7 | async-start | bytes 17825792 | tf_op jit(solution)/shard_map/all_gather | solution.py:18
  289.5 2.8 copy-start.12
  290.9 2.4 copy-start.23
  290.9 36.5 %copy-start.20 = (bf16[2048]{0:T(1024)(128)(2,1)S(1)}, bf16[2048]{0:T(1024)(128)(2,1)}, u32[]{:S(2)}) copy-start(bf16[2048]{0:T(1024)(128)(2,1)} %param.32) | copy-start | bytes 12292
  290.9 70.2 %copy-start.22 = (f32[128]{0:T(128)S(1)}, f32[128]{0:T(128)}, u32[]{:S(2)}) copy-start(f32[128]{0:T(128)} %copy-done.21) | copy-start | bytes 1540
  292.4 595.1 %all-gather.20.cloned.1.call-start = ((), (), s32[]{:S(2)}) async-start(), calls=%async_computation.5 | async-start | bytes 8912896 | tf_op jit(solution)/shard_map/all_gather | solution.py:197
  293.1 609.4 %reduce-scatter.2.cloned.1.call-start = ((), (), s32[]{:S(2)}) async-start(), calls=%async_computation.6 | async-start | bytes 786432 | tf_op jit(solution)/shard_map/reduce_scatter | solution.py:198
  376.4 3.7 copy-start.3
  377.1 4.8 copy-start.1
  745.6 34.7 %copy-start.9 = (f32[128,4,128]{2,0,1:T(8,128)S(1)}, f32[128,4,128]{2,0,1:T(8,128)}, u32[]{:S(2)}) copy-start(f32[128,4,128]{2,0,1:T(8,128)} %copy.56) | copy-start | bytes 786436
  787.2 100.3 %copy-start.13 = (f32[2048]{0:T(1024)S(1)}, f32[2048]{0:T(1024)}, u32[]{:S(2)}) copy-start(f32[2048]{0:T(1024)} %convert_element_type.130) | copy-start | bytes 24580
  (10 other events, 13.8 us)
Sparse Core Ops, SparseCore 0:
  10.1 59.9 all-gather.15
  72.9 59.1 all-gather.13
  134.9 110.6 all-gather.11
  248.2 112.9 all-gather.17
  363.8 189.9 all-gather.23
  556.4 189.1 all-gather.21
  748.3 139.1 all-gather.19
  893.1 9.3 reduce-scatter.1
where the time goes:
time: 917 us; the launch traced here: 913 us
  waiting for transfers between devices  670 us (73%)
  blocking collectives  81.3 us (9%)
  other arithmetic  57.3 us (6%)
  local copies, waits for them, and re-layouts  42.6 us (5%)
  matrix products  40.6 us (4%)
  between operations  14.6 us (2%)
    all_gather x2, waiting for transfers between devices, entering_2(): everything = jax.tree.map(lambda part: lax.all_gather(part, axis), x)  319 us
    all_gather x1, waiting for transfers between devices, body(): lax.all_gather(w_value, 'sp', axis=0, tiled=True)  111 us
    all_gather x1, waiting for transfers between devices, body(): out_whole = lax.all_gather(w_out, 'sp', axis=1, tiled=True)  98.4 us
    all_gather x1, waiting for transfers between devices, body(): lax.all_gather(w_in_key, 'sp', axis=0, tiled=True)  59.9 us
    select_n x32, other arithmetic, step(): return jax.tree.map(lambda a, b: jnp.where(reached, a, b), new, before)  46.9 us
    all_gather x1, waiting for transfers between devices, body(): lax.all_gather(w_gate, 'sp', axis=0, tiled=True)  32.5 us
    all_gather x1, waiting for transfers between devices, body(): lax.all_gather(w_read, 'sp', axis=0, tiled=True)  32.4 us
    unnamed x1, blocking collectives  31.4 us
  transfers between devices with their start and end apart: 10, of which 9 were waited for; matrix products, arithmetic and copies ran while one was open for 14% of the time, Pallas kernels for 0%

commit v1 on v0

--- a/solution.py
+++ b/solution.py
@@ -1,6 +1,11 @@
+import functools
+import math
+
 import jax
 import jax.numpy as jnp
 from jax import lax
+from jax.experimental import pallas as pl
+from jax.experimental.pallas import tpu as pltpu
 from jax.sharding import PartitionSpec as P
 
 HEAD_DIM = 64
@@ -204,6 +209,438 @@
     return lax.all_gather(own_rows, "tp", axis=0, tiled=True)
 
 
+F32 = jnp.float32
+BF16 = jnp.bfloat16
+LANES = 128
+VMEM_SPEC = pl.BlockSpec(memory_space=pltpu.VMEM)
+
+
+def greet(peers):
+    barrier = pltpu.get_barrier_semaphore()
+    for peer in peers:
+        pl.semaphore_signal(
+            barrier, inc=1, device_id=peer, device_id_type=pl.DeviceIdType.MESH
+        )
+    pl.semaphore_wait(barrier, len(peers))
+
+
+def push(src, dst, send, recv, peer):
+    copy = pltpu.make_async_remote_copy(
+        src_ref=src,
+        dst_ref=dst,
+        send_sem=send,
+        recv_sem=recv,
+        device_id=peer,
+        device_id_type=pl.DeviceIdType.MESH,
+    )
+    copy.start()
+    return copy
+
+
+def gather_kernel(n, q, nrm, wv, wg, wk, wr, ws, wo, tok, wts, wout, ts, tr, ps, pr, ss, sr, ms, mr, os, orr, ls):
+    s, t = lax.axis_index("sp"), lax.axis_index("tp")
+    z, p = s // q, s % q
+    sibling = (s, 1 - t)
+    per = n // (wk.shape[1] // LANES)
+    half = tok.shape[2]
+    depth = wv.shape[0]
+
+    def peer(k):
+        return lax.rem(s + k, n)
+
+    def at(dz, dp):
+        return lax.rem(z + dz, q) * q + lax.rem(p + dp, q)
+
+    greet([(peer(k), t) for k in range(1, n)] + [sibling])
+    rows = pl.ds(pl.multiple_of(t * half, half), half)
+    first = []
+    for dz in range(1, q):
+        first.append(push(nrm.at[rows], tok.at[s, t], ts.at[dz], tr.at[dz], (at(dz, 0), t)))
+    own = []
+    for c in range(2):
+        copy = pltpu.make_async_copy(nrm.at[pl.ds(c * half, half)], tok.at[s, c], ls.at[c])
+        copy.start()
+        own.append(copy)
+    mine = pl.ds(pl.multiple_of(s * depth, depth), depth)
+
+    def pieces(j):
+        cols = pl.ds(pl.multiple_of(j * LANES, LANES), LANES)
+        group = pl.ds(pl.multiple_of((j // per) * LANES, LANES), LANES)
+        return (wv.at[:, cols], wg.at[:, cols], wk.at[:, group], wr.at[:, group], ws.at[j])
+
+    def target(i):
+        return wts.at[mine, pl.ds(i * LANES, LANES)]
+
+    second = []
+    for dp in range(1, q):
+        second.append(push(nrm.at[rows], tok.at[s, t], ps.at[0, dp], pr.at[0, dp], (at(0, dp), t)))
+    sent = []
+    for k in range(1, n):
+        for i, piece in enumerate(pieces(peer(k))):
+            sent.append(push(piece, target(i), ms.at[k, i], mr.at[k, i], (peer(k), t)))
+    for i, piece in enumerate(pieces(s)):
+        copy = pltpu.make_async_copy(piece, target(i), ls.at[2 + i])
+        copy.start()
+        own.append(copy)
+    last = []
+    for dz in range(1, q):
+        first[dz - 1].wait_recv()
+        src = at(q - dz, 0)
+        for dp in range(1, q):
+            second.append(
+                push(tok.at[src, t], tok.at[src, t], ps.at[dz, dp], pr.at[dz, dp], (at(0, dp), t))
+            )
+        last.append(push(tok.at[src, t], tok.at[src, t], ss.at[dz, 0], sr.at[dz, 0], sibling))
+    outs = []
+    col = pl.ds(pl.multiple_of(p * LANES, LANES), LANES)
+    for dp in range(1, q):
+        outs.append(push(wo, wout.at[:, col], os.at[dp], orr.at[dp], (at(0, dp), t)))
+    copy = pltpu.make_async_copy(wo, wout.at[:, col], ls.at[7])
+    copy.start()
+    own.append(copy)
+    for dz in range(q):
+        for dp in range(1, q):
+            second[dz * (q - 1) + dp - 1].wait_recv()
+            src = at(q - dz, q - dp)
+            last.append(push(tok.at[src, t], tok.at[src, t], ss.at[dz, dp], sr.at[dz, dp], sibling))
+    for copy in own:
+        copy.wait()
+    for copy in first + second:
+        copy.wait_send()
+    for copy in sent + last + outs:
+        copy.wait()
+
+
+def gather(n, q, nrm, wv, wg, wk, wr, ws, wo):
+    dma = pltpu.SemaphoreType.DMA
+    length, width = nrm.shape
+    return pl.pallas_call(
+        functools.partial(gather_kernel, n, q),
+        out_shape=(
+            jax.ShapeDtypeStruct((n, 2, length // 2, width), BF16),
+            jax.ShapeDtypeStruct((n * wv.shape[0], 5 * LANES), BF16),
+            jax.ShapeDtypeStruct((wo.shape[0], q * LANES), BF16),
+        ),
+        in_specs=[VMEM_SPEC] * 7,
+        out_specs=(VMEM_SPEC,) * 3,
+        scratch_shapes=[
+            dma((q,)), dma((q,)), dma((q, q)), dma((q, q)), dma((q, q)), dma((q, q)),
+            dma((n, 5)), dma((n, 5)), dma((q,)), dma((q,)), dma((8,)),
+        ],
+        compiler_params=pltpu.CompilerParams(
+            collective_id=0, has_side_effects=True, vmem_limit_bytes=48 << 20
+        ),
+        name="gather",
+    )(nrm, wv, wg, wk, wr, ws, wo)
+
+
+def spread_kernel(q, nh, full, s1, r1, s2, r2, ls):
+    s, t = lax.axis_index("sp"), lax.axis_index("tp")
+    z, p = s // q, s % q
+
+    def at(dz, dp):
+        return lax.rem(z + dz, q) * q + lax.rem(p + dp, q)
+
+    def col(i):
+        return pl.ds(pl.multiple_of(i * LANES, LANES), LANES)
+
+    greet([(at(0, d), t) for d in range(1, q)] + [(at(d, 0), t) for d in range(1, q)])
+    first = []
+    for dp in range(1, q):
+        first.append(
+            push(
+                nh.at[:, lax.rem(p + dp, q)], full.at[:, :, col(s)],
+                s1.at[dp], r1.at[dp], (at(0, dp), t),
+            )
+        )
+    own = pltpu.make_async_copy(nh.at[:, p], full.at[:, :, col(s)], ls.at[0])
+    own.start()
+    second = []
+    for dz in range(1, q):
+        second.append(
+            push(nh.at[:, p], full.at[:, :, col(s)], s2.at[dz, 0], r2.at[dz, 0], (at(dz, 0), t))
+        )
+    for dp in range(1, q):
+        first[dp - 1].wait_recv()
+        got = full.at[:, :, col(at(0, q - dp))]
+        for dz in range(1, q):
+            second.append(push(got, got, s2.at[dz, dp], r2.at[dz, dp], (at(dz, 0), t)))
+    own.wait()
+    for copy in first:
+        copy.wait_send()
+    for copy in second:
+        copy.wait()
+
+
+def spread(n, q, nh):
+    dma = pltpu.SemaphoreType.DMA
+    return pl.pallas_call(
+        functools.partial(spread_kernel, q),
+        out_shape=jax.ShapeDtypeStruct((q, nh.shape[2], n * LANES), BF16),
+        in_specs=[VMEM_SPEC],
+        out_specs=VMEM_SPEC,
+        scratch_shapes=[dma((q,)), dma((q,)), dma((q, q)), dma((q, q)), dma((1,))],
+        compiler_params=pltpu.CompilerParams(collective_id=1, has_side_effects=True),
+        name="spread",
+    )(nh)
+
+
+def settle_kernel(q, part, both, s1, r1, s2, r2, ls):
+    s, t = lax.axis_index("sp"), lax.axis_index("tp")
+    z, p = s // q, s % q
+    wide = part.shape[2]
+
+    def at(dz):
+        return lax.rem(z + dz, q) * q + p
+
+    def col(i):
+        return pl.ds(pl.multiple_of(i * wide, wide), wide)
+
+    greet([(at(d), t) for d in range(1, q)] + [(s, 1 - t)])
+    first = []
+    for dz in range(1, q):
+        first.append(
+            push(
+                part.at[lax.rem(z + dz, q)], both.at[t, :, col(z)],
+                s1.at[dz], r1.at[dz], (at(dz), t),
+            )
+        )
+    own = pltpu.make_async_copy(part.at[z], both.at[t, :, col(z)], ls.at[0])
+    own.start()
+    second = [push(part.at[z], both.at[t, :, col(z)], s2.at[0], r2.at[0], (s, 1 - t))]
+    for dz in range(1, q):
+        first[dz - 1].wait_recv()
+        got = both.at[t, :, col(lax.rem(z + q - dz, q))]
+        second.append(push(got, got, s2.at[dz], r2.at[dz], (s, 1 - t)))
+    own.wait()
+    for copy in first:
+        copy.wait_send()
+    for copy in second:
+        copy.wait()
+
+
+def exchange(q, part):
+    dma = pltpu.SemaphoreType.DMA
+    return pl.pallas_call(
+        functools.partial(settle_kernel, q),
+        out_shape=jax.ShapeDtypeStruct((2, part.shape[1], q * part.shape[2]), BF16),
+        in_specs=[VMEM_SPEC],
+        out_specs=VMEM_SPEC,
+        scratch_shapes=[dma((q,)), dma((q,)), dma((q,)), dma((q,)), dma((1,))],
+        compiler_params=pltpu.CompilerParams(collective_id=2, has_side_effects=True),
+        name="exchange",
+    )(part)
+
+
+def silu(x):
+    return x * jax.nn.sigmoid(x)
+
+
+def mix_kernel(tok, wts, taps, offsets, rates, gain, out, raw, gate, pre, vals, keys, reads, cums, yy, injf, injb):
+    seq = tok.shape[0]
+    rows = 2 * BLOCK
+    wide = 3 * LANES
+    blocks = seq // BLOCK
+    raw[0:8, :] = jnp.zeros((8, wide), F32)
+    raw[seq + 8 : seq + 16, :] = jnp.zeros((8, wide), F32)
+
+    @pl.loop(0, seq // rows)
+    def _(i):
+        r0 = pl.multiple_of(i * rows, rows)
+        got = jnp.dot(tok[pl.ds(r0, rows), :], wts[...], preferred_element_type=F32).astype(BF16)
+        for a, b in ((0, 0), (2, 1), (3, 2)):
+            raw[pl.ds(r0 + 8, rows), b * LANES : (b + 1) * LANES] = got[
+                :, a * LANES : (a + 1) * LANES
+            ].astype(F32)
+        gate[pl.ds(r0, rows), :] = got[:, LANES : 2 * LANES]
+        x = got[:, 4 * LANES :].astype(F32) + offsets[...]
+        pre[pl.ds(r0, rows), :] = jnp.maximum(x, 0.0) + jnp.log1p(jnp.exp(-jnp.abs(x)))
+
+    @pl.loop(0, blocks)
+    def _(i):
+        r0 = pl.multiple_of(i * BLOCK, BLOCK)
+        for b, dst in enumerate((vals, keys, reads)):
+            window = raw[pl.ds(r0, BLOCK + 16), b * LANES : (b + 1) * LANES]
+            total = jnp.zeros((BLOCK, LANES), F32)
+            for k in range(KERNEL):
+                lo = 8 - (KERNEL - 1) // 2 + k
+                total = total + window[lo : lo + BLOCK] * taps[k : k + 1, b * LANES : (b + 1) * LANES]
+            dst[pl.ds(r0, BLOCK), :] = silu(total).astype(BF16)
+
+    ri = lax.broadcasted_iota(jnp.int32, (BLOCK, BLOCK), 0)
+    ci = lax.broadcasted_iota(jnp.int32, (BLOCK, BLOCK), 1)
+    low = ri >= ci
+    diag = ri == ci
+    fwd = ci < 2
+    left = ci < HEAD_DIM
+    lower = jnp.where(low, 1.0, 0.0).astype(F32)
+    upper = jnp.where(ri <= ci, 1.0, 0.0).astype(F32)
+
+    @pl.loop(0, blocks)
+    def _(i):
+        r0 = pl.multiple_of(i * BLOCK, BLOCK)
+        at = pl.ds(r0, BLOCK)
+        st = pre[at, :]
+        ld = -rates[...] * st
+        c = jnp.where(
+            fwd,
+            jnp.dot(lower, ld, precision=FULL_PRECISION, preferred_element_type=F32),
+            jnp.dot(upper, ld, precision=FULL_PRECISION, preferred_element_type=F32),
+        )
+        cums[at, :] = c
+        ct = c.T
+        stt = st.T
+        key, read, val = keys[at, :], reads[at, :], vals[at, :]
+        val32 = val.astype(F32)
+        score = lax.dot_general(read, key, (((1,), (1,)), ((), ())), preferred_element_type=F32)
+        total = jnp.zeros((BLOCK, LANES), F32)
+        for h in range(2):
+            gap = jnp.where(low, c[:, h : h + 1] - ct[h : h + 1, :], c[:, h + 2 : h + 3] - ct[h + 2 : h + 3, :])
+            sb = stt[h + 2 : h + 3, :]
+            e = jnp.exp(gap) * jnp.where(low, stt[h : h + 1, :], sb) + jnp.where(diag, sb, 0.0)
+            side = left if h == 0 else jnp.logical_not(left)
+            own = jnp.where(side, val32, 0.0).astype(BF16)
+            total = total + jnp.dot((score * e).astype(BF16), own, preferred_element_type=F32)
+        yy[at, :] = total
+        c_end = jnp.where(fwd[0:1], c[BLOCK - 1 : BLOCK, :], c[0:1, :])
+        weighting = jnp.exp(c_end - c) * st
+        key_t = key.astype(F32).T.astype(BF16)
+        for d, dst in ((0, injf), (1, injb)):
+            w = jnp.where(left, weighting[:, 2 * d : 2 * d + 1], weighting[:, 2 * d + 1 : 2 * d + 2])
+            scaled = (val32 * w).astype(BF16)
+            dst[i] = jnp.dot(key_t, scaled, preferred_element_type=F32)
+
+    def carry(i, state, d, inj):
+        r0 = pl.multiple_of(i * BLOCK, BLOCK)
+        at = pl.ds(r0, BLOCK)
+        ec = jnp.exp(cums[at, :])
+        grown = jnp.where(left, ec[:, 2 * d : 2 * d + 1], ec[:, 2 * d + 1 : 2 * d + 2])
+        high = state.astype(BF16)
+        rest = (state - high.astype(F32)).astype(BF16)
+        read = reads[at, :]
+        add = jnp.dot(read, high, preferred_element_type=F32) + jnp.dot(
+            read, rest, preferred_element_type=F32
+        )
+        yy[at, :] = yy[at, :] + add * grown
+        end = grown[BLOCK - 1 : BLOCK, :] if d == 0 else grown[0:1, :]
+        return state * end + inj[i]
+
+    def both(i, states):
+        return (
+            carry(i, states[0], 0, injf),
+            carry(blocks - 1 - i, states[1], 1, injb),
+        )
+
+    zero = jnp.zeros((STATE, LANES), F32)
+    lax.fori_loop(0, blocks, both, (zero, zero))
+
+    @pl.loop(0, blocks)
+    def _(i):
+        r0 = pl.multiple_of(i * BLOCK, BLOCK)
+        at = pl.ds(r0, BLOCK)
+        g = yy[at, :] * silu(gate[at, :].astype(F32))
+        sq = g * g
+        m0 = jnp.sum(jnp.where(left, sq, 0.0), -1, keepdims=True) / HEAD_DIM
+        m1 = jnp.sum(jnp.where(left, 0.0, sq), -1, keepdims=True) / HEAD_DIM
+        scale = jnp.where(left, lax.rsqrt(m0 + EPSILON), lax.rsqrt(m1 + EPSILON))
+        out[at, :] = (g * scale * gain[...]).astype(BF16)
+
+
+def mix(tok, wts, taps, offsets, rates, gain):
+    seq = tok.shape[0]
+    vm = pltpu.VMEM
+    return pl.pallas_call(
+        mix_kernel,
+        out_shape=jax.ShapeDtypeStruct((seq, LANES), BF16),
+        in_specs=[VMEM_SPEC] * 6,
+        out_specs=VMEM_SPEC,
+        scratch_shapes=[
+            vm((seq + 16, 3 * LANES), F32),
+            vm((seq, LANES), BF16),
+            vm((seq, LANES), F32),
+            vm((seq, LANES), BF16),
+            vm((seq, LANES), BF16),
+            vm((seq, LANES), BF16),
+            vm((seq, LANES), F32),
+            vm((seq, LANES), F32),
+            vm((seq // BLOCK, STATE, LANES), F32),
+            vm((seq // BLOCK, STATE, LANES), F32),
+        ],
+        compiler_params=pltpu.CompilerParams(vmem_limit_bytes=48 << 20),
+        name="mix",
+    )(tok, wts, taps, offsets, rates, gain)
+
+
+def own_lanes(fwd, bwd, n):
+    both = jnp.stack([fwd.reshape(fwd.shape[0], n, -1), bwd.reshape(bwd.shape[0], n, -1)], 2)
+    both = both.reshape(fwd.shape[0], n, -1)
+    both = jnp.pad(both, ((0, 0), (0, 0), (0, LANES - both.shape[2])))
+    return both.transpose(1, 0, 2)
+
+
+def headwise(
+    n,
+    q,
+    tokens,
+    in_gain,
+    w_value,
+    w_gate,
+    w_in_key,
+    w_read,
+    w_step_fwd,
+    w_step_bwd,
+    conv_value,
+    conv_key,
+    conv_read,
+    step_bias,
+    rate,
+    norm_gain,
+    w_out,
+):
+    s = lax.axis_index("sp")
+    group = s // (n // (w_in_key.shape[1] // LANES))
+    nrm = normalize(tokens.astype(F32), in_gain.astype(F32)).astype(BF16)
+    steps = own_lanes(w_step_fwd, w_step_bwd, n)
+    tok, wts, wout = gather(n, q, nrm, w_value, w_gate, w_in_key, w_read, steps, w_out)
+    seq = n * nrm.shape[0]
+
+    def cut(x, j):
+        return lax.dynamic_slice_in_dim(x, j * LANES, LANES, 1)
+
+    taps = jnp.concatenate([cut(conv_value, s), cut(conv_key, group), cut(conv_read, group)], 1)
+    small = own_lanes(
+        jnp.stack([step_bias[0], rate[0]]), jnp.stack([step_bias[1], rate[1]]), n
+    )
+    small = lax.dynamic_index_in_dim(small, s, 0, keepdims=False)
+    gain = lax.dynamic_slice_in_dim(norm_gain, s * LANES, LANES, 0).astype(F32)[None]
+    nh = mix(
+        tok.reshape(seq, nrm.shape[1]), wts, taps.astype(F32), small[0:1], small[1:2], gain
+    )
+    full = spread(n, q, nh.reshape(q, q, nrm.shape[0], LANES))
+    part = jnp.einsum("zrk,kc->zrc", full, wout, preferred_element_type=F32).astype(BF16)
+    halves = exchange(q, part)
+    return (halves[0].astype(F32) + halves[1].astype(F32)).astype(BF16)
+
+
+def whole_heads(mesh):
+    n, q = mesh.shape["sp"], math.isqrt(mesh.shape["sp"])
+
+    def run(*args):
+        cols, keys = args[2].shape[1], args[4].shape[1]
+        ready = (
+            q * q == n
+            and mesh.shape["tp"] == 2
+            and cols == n * LANES
+            and args[14].shape[1] == LANES
+            and keys % LANES == 0
+            and n % (keys // LANES) == 0
+            and args[0].shape[0] == BLOCK
+        )
+        return headwise(n, q, *args) if ready else body(*args)
+
+    return run
+
+
 def solution(mesh):
     in_specs = (
         P("sp", None),
@@ -223,4 +660,4 @@
         P("tp", "sp"),
     )
     out_specs = P("sp", None)
-    return jax.shard_map(body, mesh=mesh, in_specs=in_specs, out_specs=out_specs, check_vma=False)
+    return jax.shard_map(whole_heads(mesh), mesh=mesh, in_specs=in_specs, out_specs=out_specs, check_vma=False)

time: 917 us -> 231 us (0.25)
  waiting for transfers between devices: 670 us -> 0 us
  Pallas kernels: 0 us -> 212 us
  blocking collectives: 81.3 us -> 0 us
  other arithmetic: 57.3 us -> 6.94 us
  matrix products: 40.6 us -> 3.63 us
  local copies, waits for them, and re-layouts: 42.6 us -> 5.65 us
  between operations: 14.6 us -> 0.22 us
    all_gather x7 -> x0, waiting for transfers between devices: 654 us -> none  [the longest x2 319 us: entering_2(): everything = jax.tree.map(lambda part: lax.all_gather(part, axis), x)]
    pallas_call x0 -> x4, Pallas kernels: none -> 212 us  [the longest x1 111 us: gather(): pl.pallas_call(functools.partial(gather_kernel, n, q), out_shape=(jax.Sha...]
    all_gather x3 -> x0, blocking collectives: 50 us -> none  [the longest x1 24.5 us: body(): lax.all_gather(w_step_fwd, 'sp', axis=0, tiled=True)]
    select_n x32 -> x0, other arithmetic: 46.9 us -> none  [step(): return jax.tree.map(lambda a, b: jnp.where(reached, a, b), new, before)]
    dot_general x15 -> x1, matrix products: 40.6 us -> 3.63 us  [headwise(): jnp.einsum('zrk,kc->zrc', full, wout, preferred_element_type=F32)]
    unnamed x1 -> x0, blocking collectives: 31.4 us -> none
    mul x35 -> x0, local copies, waits for them, and re-layouts: 23.7 us -> none  [the longest x32 21.9 us: chain(): after_pair[0][:, None, None] * before_pair[1] + after_pair[1]]
    reduce_scatter x1 -> x0, waiting for transfers between devices: 9.54 us -> none  [body(): lax.psum_scatter(jnp.dot(normed_heads, out_whole, preferred_element_type=...]
  transfers between devices with their start and end apart: 10 -> 0, of which waited for: 9 -> 0; matrix products, arithmetic and copies ran while one was open for 14% -> 0% of each run, Pallas kernels for 0% -> 0%
where the time goes in v1:
time: 231 us; the launch traced here: 228 us
  Pallas kernels  212 us (92%)
  other arithmetic  6.94 us (3%)
  local copies, waits for them, and re-layouts  5.65 us (2%)
  matrix products  3.63 us (2%)
    pallas_call x1, Pallas kernels, gather(): pl.pallas_call(functools.partial(gather_kernel, n, q), out_shape=(jax.Sha...  111 us
    pallas_call x1, Pallas kernels, spread(): pl.pallas_call(functools.partial(spread_kernel, q), out_shape=jax.ShapeDt...  51.2 us
    pallas_call x1, Pallas kernels, mix(): pl.pallas_call(mix_kernel, out_shape=jax.ShapeDtypeStruct((seq, LANES), B...  31.3 us
    pallas_call x1, Pallas kernels, exchange(): pl.pallas_call(functools.partial(settle_kernel, q), out_shape=jax.ShapeDt...  18.3 us

profile of v1, /device:TPU:19, one launch (start us, length us, event | category | flops | bytes accessed | tf_op | source)
XLA Modules:
  0.0 228.4 jit_solution(18190906016316078884)
XLA Ops:
  0.0 0.8 convert_element_type.35
  0.9 1.2 fusion.5
  2.1 1.2 fusion.7.nrm
  3.3 0.7 pad_maximum_fusion
  4.1 0.3 copy.25
  4.4 0.0 copy-start.10
  4.4 0.0 copy-start.11
  4.4 0.1 pad_bitcast_fusion.ws
  4.6 111.1 %gather.1 = (bf16[16,2,64,2048]{3,2,1,0:T(8,128)(2,1)}, bf16[2048,640]{1,0:T(8,128)(2,1)}, bf16[2048,512]{1,0:T(8,128)(2,1)S(1)}) custom-call(bf16[128,2048]{1,0:T(8,128)(2,1)S(1)} %fusion.7.nrm, bf16[128,2048]{1,0:T(8,128)(2,1)S(1)} %copy-done.3, bf16[128,2048]{1,0:T(8,128)(2,1)S(1)} %copy-done.4, bf16[128,512]{1,0:T(8,128)(2,1)S(1)} %copy-done.6, ...), custom_call_target="tpu_custom_call" | custom-call | tf_op jit(solution)/shard_map/gather/pallas_call | solution.py:317
  115.8 1.4 copy-done.8
  117.2 0.7 constant_dynamic-slice_fusion
  117.9 0.1 stack_reshape.15
  118.0 0.1 copy.27
  118.1 0.1 stack_reshape.14
  118.2 0.1 copy.26
  118.3 0.2 dynamic-slice_reduce_fusion
  118.5 0.8 bitcast_convert_fusion.gain
  119.3 1.7 copy-done.1
  121.0 31.3 %mix.1 = bf16[2048,128]{1,0:T(8,128)(2,1)S(1)} custom-call(bf16[2048,2048]{1,0:T(8,128)(2,1)} %bitcast.25, bf16[2048,640]{1,0:T(8,128)(2,1)S(1)} %copy-done.1, f32[5,384]{1,0:T(8,128)S(1)} %maximum_convert_fusion.taps, f32[1,128]{1,0:T(1,128)S(1)} %get-tuple-element.12.offsets, f32[1,128]{1,0:T(1,128)S(1)} %get-tuple-element.11.rates, ...), custom_call_target="tpu_custom_call" | custom-call | tf_op jit(solution)/shard_map/mix/pallas_call | solution.py:552
  152.3 0.8 copy-done.2
  153.1 51.2 %spread.1 = bf16[4,128,2048]{2,1,0:T(8,128)(2,1)} custom-call(bf16[4,4,128,128]{3,2,1,0:T(8,128)(2,1)} %bitcast.24), custom_call_target="tpu_custom_call" | custom-call | tf_op jit(solution)/shard_map/spread/pallas_call | solution.py:377
  204.3 3.6 %fusion.2.part = bf16[4,128,512]{2,1,0:T(8,128)(2,1)} fusion(bf16[4,128,2048]{2,1,0:T(8,128)(2,1)} %spread.1, bf16[2048,512]{1,0:T(8,128)(2,1)S(1)} %copy-done.9), kind=kOutput, calls=%fused_computation.4 | convolution fusion | flops 1074003968 | bytes 4718592 | tf_op jit(solution)/shard_map/zrk,kc->zrc/dot_general | solution.py:620
  208.0 18.3 %exchange.1 = bf16[2,128,2048]{2,1,0:T(8,128)(2,1)} custom-call(bf16[4,128,512]{2,1,0:T(8,128)(2,1)} %fusion.2.part), custom_call_target="tpu_custom_call" | custom-call | tf_op jit(solution)/shard_map/exchange/pallas_call | solution.py:424
  226.3 2.1 fusion.8
  (28 shorter events, 0.1 us)
Async XLA Ops:
  0.0 117.9 %copy-start = (bf16[5,2048]{1,0:T(8,128)(2,1)S(1)}, bf16[5,2048]{1,0:T(8,128)(2,1)}, u32[]{:S(2)}) copy-start(bf16[5,2048]{1,0:T(8,128)(2,1)} %param.23) | copy-start | bytes 61444
  0.0 4.6 %copy-start.3 = (bf16[128,2048]{1,0:T(8,128)(2,1)S(1)}, bf16[128,2048]{1,0:T(8,128)(2,1)}, u32[]{:S(2)}) copy-start(bf16[128,2048]{1,0:T(8,128)(2,1)} %wv.1) | copy-start | bytes 1572868
  0.0 4.6 %copy-start.4 = (bf16[128,2048]{1,0:T(8,128)(2,1)S(1)}, bf16[128,2048]{1,0:T(8,128)(2,1)}, u32[]{:S(2)}) copy-start(bf16[128,2048]{1,0:T(8,128)(2,1)} %wg.1) | copy-start | bytes 1572868
  0.0 4.6 %copy-start.6 = (bf16[128,512]{1,0:T(8,128)(2,1)S(1)}, bf16[128,512]{1,0:T(8,128)(2,1)}, u32[]{:S(2)}) copy-start(bf16[128,512]{1,0:T(8,128)(2,1)} %wk.1) | copy-start | bytes 393220
  0.0 4.6 %copy-start.7 = (bf16[128,512]{1,0:T(8,128)(2,1)S(1)}, bf16[128,512]{1,0:T(8,128)(2,1)}, u32[]{:S(2)}) copy-start(bf16[128,512]{1,0:T(8,128)(2,1)} %wr.1) | copy-start | bytes 393220
  0.0 4.6 %copy-start.5 = (bf16[2048,128]{1,0:T(8,128)(2,1)S(1)}, bf16[2048,128]{1,0:T(8,128)(2,1)}, u32[]{:S(2)}) copy-start(bf16[2048,128]{1,0:T(8,128)(2,1)} %wo.1) | copy-start | bytes 1572868
  4.4 113.5 %copy-start.10 = (f32[2,32]{1,0:T(2,128)S(1)}, f32[2,32]{1,0:T(2,128)}, u32[]{:S(2)}) copy-start(f32[2,32]{1,0:T(2,128)} %param.27) | copy-start | bytes 772
  4.4 113.5 %copy-start.11 = (f32[2,32]{1,0:T(2,128)S(1)}, f32[2,32]{1,0:T(2,128)}, u32[]{:S(2)}) copy-start(f32[2,32]{1,0:T(2,128)} %param.26) | copy-start | bytes 772
  115.8 1.4 copy-start.8
  119.3 1.7 copy-start.1
  152.3 0.8 copy-start.2
  153.1 51.2 %copy-start.9 = (bf16[2048,512]{1,0:T(8,128)(2,1)S(1)}, bf16[2048,512]{1,0:T(8,128)(2,1)}, u32[]{:S(2)}) copy-start(bf16[2048,512]{1,0:T(8,128)(2,1)} %copy-done.8) | copy-start | bytes 6291460

commit v2 on v0

--- a/solution.py
+++ b/solution.py
@@ -1,6 +1,11 @@
+import functools
+import math
+
 import jax
 import jax.numpy as jnp
 from jax import lax
+from jax.experimental import pallas as pl
+from jax.experimental.pallas import tpu as pltpu
 from jax.sharding import PartitionSpec as P
 
 HEAD_DIM = 64
@@ -204,6 +209,415 @@
     return lax.all_gather(own_rows, "tp", axis=0, tiled=True)
 
 
+F32 = jnp.float32
+BF16 = jnp.bfloat16
+LANES = 128
+VMEM_SPEC = pl.BlockSpec(memory_space=pltpu.VMEM)
+
+
+def greet(peers):
+    barrier = pltpu.get_barrier_semaphore()
+    for peer in peers:
+        pl.semaphore_signal(
+            barrier, inc=1, device_id=peer, device_id_type=pl.DeviceIdType.MESH
+        )
+    pl.semaphore_wait(barrier, len(peers))
+
+
+def push(src, dst, send, recv, peer):
+    copy = pltpu.make_async_remote_copy(
+        src_ref=src,
+        dst_ref=dst,
+        send_sem=send,
+        recv_sem=recv,
+        device_id=peer,
+        device_id_type=pl.DeviceIdType.MESH,
+    )
+    copy.start()
+    return copy
+
+
+def silu(x):
+    return x * jax.nn.sigmoid(x)
+
+
+def whole_kernel(
+    n, q, nrm, wv, wg, wk, wr, ws, wo, taps, offsets, rates, gain, both,
+    tok, wts, wst, wout, raw, gate, pre, vals, keys, reads, cums, yy, injf, injb, nh, full, part,
+    tzs, tzr, tps, tpr, tss, tsr, kzs, kzr, kps, kpr, vs, vr, ss, sr, os, orr,
+    as_, ar, bs, br, es, er, fs, fr, ls,
+):
+    s, t = lax.axis_index("sp"), lax.axis_index("tp")
+    z, p = s // q, s % q
+    sibling = (s, 1 - t)
+    half = tok.shape[2]
+    depth = wv.shape[0]
+    blocks = tok.shape[0] * 2 * half // BLOCK
+
+    def at(dz, dp):
+        return lax.rem(z + dz, q) * q + lax.rem(p + dp, q)
+
+    def span(i, size):
+        return pl.ds(pl.multiple_of(i * size, size), size)
+
+    greet([(lax.rem(s + k, n), t) for k in range(1, n)] + [sibling])
+    done, sent = [], []
+
+    def local(src, dst, i):
+        copy = pltpu.make_async_copy(src, dst, ls.at[i])
+        copy.start()
+        return copy
+
+    mine = span(s, depth)
+    rows = span(t, half)
+    kcol, rcol = pl.ds(2 * LANES, LANES), pl.ds(3 * LANES, LANES)
+    first, keyz = [], []
+    for dz in range(1, q):
+        first.append(push(nrm.at[rows], tok.at[s, t], tzs.at[dz], tzr.at[dz], (at(dz, 0), t)))
+    for dz in range(1, q):
+        grp = span(lax.rem(z + dz, q), LANES)
+        keyz.append(
+            [
+                push(w.at[:, grp], wts.at[mine, col], kzs.at[dz, i], kzr.at[dz, i], (at(dz, 0), t))
+                for i, (w, col) in enumerate(((wk, kcol), (wr, rcol)))
+            ]
+        )
+    plane, keyp = {}, []
+    for dp in range(1, q):
+        plane[0, dp] = push(nrm.at[rows], tok.at[s, t], tps.at[0, dp], tpr.at[0, dp], (at(0, dp), t))
+    for dp in range(1, q):
+        for i, (w, col) in enumerate(((wk, kcol), (wr, rcol))):
+            keyp.append(
+                push(
+                    w.at[:, span(z, LANES)], wts.at[mine, col],
+                    kps.at[i * q, dp], kpr.at[i * q, dp], (at(0, dp), t),
+                )
+            )
+    locals_ = [
+        local(nrm.at[pl.ds(0, half)], tok.at[s, 0], 0),
+        local(nrm.at[pl.ds(half, half)], tok.at[s, 1], 1),
+        local(wk.at[:, span(z, LANES)], wts.at[mine, kcol], 2),
+        local(wr.at[:, span(z, LANES)], wts.at[mine, rcol], 3),
+        local(wv.at[:, mine], wts.at[mine, pl.ds(0, LANES)], 4),
+        local(wg.at[:, mine], wts.at[mine, pl.ds(LANES, LANES)], 5),
+        local(ws.at[s], wst.at[pl.ds(0, ws.shape[1]), mine], 6),
+    ]
+    weights = []
+    for k in range(1, n):
+        j = lax.rem(s + k, n)
+        cols = span(j, LANES)
+        for i, w in enumerate((wv, wg)):
+            weights.append(
+                push(w.at[:, cols], wts.at[mine, pl.ds(i * LANES, LANES)], vs.at[k, i], vr.at[k, i], (j, t))
+            )
+        weights.append(
+            push(ws.at[j], wst.at[pl.ds(0, ws.shape[1]), mine], ss.at[k], sr.at[k], (j, t))
+        )
+    swaps = {}
+
+    def swap(dz, dp):
+        src = at(q - dz, q - dp)
+        swaps[dz, dp] = push(tok.at[src, t], tok.at[src, t], tss.at[dz, dp], tsr.at[dz, dp], sibling)
+
+    for dz in range(1, q):
+        src = at(q - dz, 0)
+        first[dz - 1].wait_recv()
+        for dp in range(1, q):
+            plane[dz, dp] = push(tok.at[src, t], tok.at[src, t], tps.at[dz, dp], tpr.at[dz, dp], (at(0, dp), t))
+        swap(dz, 0)
+        for copy in keyz[dz - 1]:
+            copy.wait_recv()
+        got = wts.at[span(src, depth), pl.ds(2 * LANES, 2 * LANES)]
+        for dp in range(1, q):
+            keyp.append(push(got, got, kps.at[dz, dp], kpr.at[dz, dp], (at(0, dp), t)))
+    outs = []
+    for dz in range(1, q):
+        outs.append(push(wo, wout.at[:, span(z, LANES)], os.at[dz], orr.at[dz], (at(dz, 0), t)))
+    locals_.append(local(wo, wout.at[:, span(z, LANES)], 7))
+
+    wst[ws.shape[1] :, :] = jnp.zeros((LANES - ws.shape[1], wst.shape[1]), BF16)
+    seq = blocks * BLOCK
+    wide = 3 * LANES
+    raw[0:8, :] = jnp.zeros((8, wide), F32)
+    raw[seq + 8 : seq + 16, :] = jnp.zeros((8, wide), F32)
+    for copy in locals_:
+        copy.wait()
+    for copy in weights + keyp:
+        copy.wait_recv()
+
+    def project(plane_index):
+        @pl.loop(0, q // 2)
+        def _(i):
+            chip = plane_index * q + 2 * i
+            r0 = pl.multiple_of(chip * BLOCK, 2 * BLOCK)
+            at2 = pl.ds(r0, 2 * BLOCK)
+            x = tok[pl.ds(chip, 2)].reshape(2 * BLOCK, tok.shape[3])
+            got = jnp.dot(x, wts[...], preferred_element_type=F32).astype(BF16)
+            for i_, b_ in ((0, 0), (2, 1), (3, 2)):
+                raw[pl.ds(r0 + 8, 2 * BLOCK), b_ * LANES : (b_ + 1) * LANES] = got[
+                    :, i_ * LANES : (i_ + 1) * LANES
+                ].astype(F32)
+            gate[at2, :] = got[:, LANES : 2 * LANES]
+            u = lax.dot_general(x, wst[...], (((1,), (1,)), ((), ())), preferred_element_type=F32)
+            u = u.astype(BF16).astype(F32) + offsets[...]
+            pre[at2, :] = jnp.maximum(u, 0.0) + jnp.log1p(jnp.exp(-jnp.abs(u)))
+
+    for dz in range(q):
+        for dp in range(1, q):
+            plane[dz, dp].wait_recv()
+            swap(dz, dp)
+        for dp in range(q):
+            if (dz, dp) != (0, 0):
+                swaps[dz, dp].wait_recv()
+        project(lax.rem(z + q - dz, q))
+
+    @pl.loop(0, blocks)
+    def _(i):
+        r0 = pl.multiple_of(i * BLOCK, BLOCK)
+        for b, dst in enumerate((vals, keys, reads)):
+            window = raw[pl.ds(r0, BLOCK + 16), b * LANES : (b + 1) * LANES]
+            total = jnp.zeros((BLOCK, LANES), F32)
+            for k in range(KERNEL):
+                lo = 8 - (KERNEL - 1) // 2 + k
+                total = total + window[lo : lo + BLOCK] * taps[k : k + 1, b * LANES : (b + 1) * LANES]
+            dst[pl.ds(r0, BLOCK), :] = silu(total).astype(BF16)
+
+    ri = lax.broadcasted_iota(jnp.int32, (BLOCK, BLOCK), 0)
+    ci = lax.broadcasted_iota(jnp.int32, (BLOCK, BLOCK), 1)
+    low = ri >= ci
+    diag = ri == ci
+    fwd = ci < 2
+    left = ci < HEAD_DIM
+    lower = jnp.where(low, 1.0, 0.0).astype(F32)
+    upper = jnp.where(ri <= ci, 1.0, 0.0).astype(F32)
+
+    @pl.loop(0, blocks)
+    def _(i):
+        r0 = pl.multiple_of(i * BLOCK, BLOCK)
+        here = pl.ds(r0, BLOCK)
+        st = pre[here, :]
+        ld = -rates[...] * st
+        c = jnp.where(
+            fwd,
+            jnp.dot(lower, ld, precision=FULL_PRECISION, preferred_element_type=F32),
+            jnp.dot(upper, ld, precision=FULL_PRECISION, preferred_element_type=F32),
+        )
+        cums[here, :] = c
+        ct = c.T
+        stt = st.T
+        key, read, val = keys[here, :], reads[here, :], vals[here, :]
+        val32 = val.astype(F32)
+        score = lax.dot_general(read, key, (((1,), (1,)), ((), ())), preferred_element_type=F32)
+        total = jnp.zeros((BLOCK, LANES), F32)
+        for h in range(2):
+            gap = jnp.where(low, c[:, h : h + 1] - ct[h : h + 1, :], c[:, h + 2 : h + 3] - ct[h + 2 : h + 3, :])
+            sb = stt[h + 2 : h + 3, :]
+            e = jnp.exp(gap) * jnp.where(low, stt[h : h + 1, :], sb) + jnp.where(diag, sb, 0.0)
+            side = left if h == 0 else jnp.logical_not(left)
+            own = jnp.where(side, val32, 0.0).astype(BF16)
+            total = total + jnp.dot((score * e).astype(BF16), own, preferred_element_type=F32)
+        yy[here, :] = total
+        c_end = jnp.where(fwd[0:1], c[BLOCK - 1 : BLOCK, :], c[0:1, :])
+        weighting = jnp.exp(c_end - c) * st
+        key_t = key.astype(F32).T.astype(BF16)
+        for d, dst in ((0, injf), (1, injb)):
+            w = jnp.where(left, weighting[:, 2 * d : 2 * d + 1], weighting[:, 2 * d + 1 : 2 * d + 2])
+            scaled = (val32 * w).astype(BF16)
+            dst[i] = jnp.dot(key_t, scaled, preferred_element_type=F32)
+
+    def carry(i, state, d, inj):
+        r0 = pl.multiple_of(i * BLOCK, BLOCK)
+        here = pl.ds(r0, BLOCK)
+        ec = jnp.exp(cums[here, :])
+        grown = jnp.where(left, ec[:, 2 * d : 2 * d + 1], ec[:, 2 * d + 1 : 2 * d + 2])
+        high = state.astype(BF16)
+        rest = (state - high.astype(F32)).astype(BF16)
+        read = reads[here, :]
+        add = jnp.dot(read, high, preferred_element_type=F32) + jnp.dot(
+            read, rest, preferred_element_type=F32
+        )
+        yy[here, :] = yy[here, :] + add * grown
+        end = grown[BLOCK - 1 : BLOCK, :] if d == 0 else grown[0:1, :]
+        return state * end + inj[i]
+
+    def advance(i, states):
+        return (
+            carry(i, states[0], 0, injf),
+            carry(blocks - 1 - i, states[1], 1, injb),
+        )
+
+    zero = jnp.zeros((STATE, LANES), F32)
+    lax.fori_loop(0, blocks, advance, (zero, zero))
+
+    def finish(i):
+        r0 = pl.multiple_of(i * BLOCK, BLOCK)
+        here = pl.ds(r0, BLOCK)
+        g = yy[here, :] * silu(gate[here, :].astype(F32))
+        sq = g * g
+        m0 = jnp.sum(jnp.where(left, sq, 0.0), -1, keepdims=True) / HEAD_DIM
+        m1 = jnp.sum(jnp.where(left, 0.0, sq), -1, keepdims=True) / HEAD_DIM
+        scale = jnp.where(left, lax.rsqrt(m0 + EPSILON), lax.rsqrt(m1 + EPSILON))
+        nh[here, :] = (g * scale * gain[...]).astype(BF16)
+
+    away = []
+    for dz in range(1, q + 1):
+        to = lax.rem(z + dz, q)
+
+        @pl.loop(0, q)
+        def _(i):
+            finish(to * q + i)
+
+        if dz < q:
+            away.append(
+                push(nh.at[span(to, q * BLOCK)], full.at[:, mine], as_.at[dz], ar.at[dz], (at(dz, 0), t))
+            )
+    near = {}
+    keep = local(nh.at[span(z, q * BLOCK)], full.at[:, mine], 8)
+    for dp in range(1, q):
+        near[0, dp] = push(
+            nh.at[span(z, q * BLOCK)], full.at[:, mine], bs.at[0, dp], br.at[0, dp], (at(0, dp), t)
+        )
+    for dz in range(1, q):
+        away[dz - 1].wait_recv()
+        got = full.at[:, span(at(q - dz, 0), LANES)]
+        for dp in range(1, q):
+            near[dz, dp] = push(got, got, bs.at[dz, dp], br.at[dz, dp], (at(0, dp), t))
+    keep.wait()
+    for copy in outs + list(near.values()):
+        copy.wait_recv()
+    legs = []
+    for dp in range(1, q + 1):
+        to = lax.rem(p + dp, q)
+        part[to] = jnp.dot(full[span(to, BLOCK), :], wout[...], preferred_element_type=F32).astype(BF16)
+    for dp in range(1, q):
+        to = lax.rem(p + dp, q)
+        legs.append(push(part.at[to], both.at[t, p], es.at[dp], er.at[dp], (at(0, dp), t)))
+    across = [push(part.at[p], both.at[t, p], fs.at[0], fr.at[0], sibling)]
+    keep = local(part.at[p], both.at[t, p], 9)
+    for dp in range(1, q):
+        legs[dp - 1].wait_recv()
+        got = both.at[t, lax.rem(p + q - dp, q)]
+        across.append(push(got, got, fs.at[dp], fr.at[dp], sibling))
+    keep.wait()
+    for copy in across:
+        copy.wait()
+    flat = [copy for pair in keyz for copy in pair]
+    for copy in first + flat + list(plane.values()) + keyp + weights + list(swaps.values()):
+        copy.wait_send()
+    for copy in outs + away + list(near.values()) + legs:
+        copy.wait_send()
+
+
+def whole(n, q, nrm, wv, wg, wk, wr, ws, wo, taps, offsets, rates, gain):
+    dma = pltpu.SemaphoreType.DMA
+    vm = pltpu.VMEM
+    depth = nrm.shape[0]
+    width = nrm.shape[1]
+    seq = n * depth
+    return pl.pallas_call(
+        functools.partial(whole_kernel, n, q),
+        out_shape=jax.ShapeDtypeStruct((2, q, BLOCK, q * LANES), BF16),
+        in_specs=[VMEM_SPEC] * 11,
+        out_specs=VMEM_SPEC,
+        scratch_shapes=[
+            vm((n, 2, depth // 2, width), BF16),
+            vm((width, 4 * LANES), BF16),
+            vm((LANES, width), BF16),
+            vm((wo.shape[0], q * LANES), BF16),
+            vm((seq + 16, 3 * LANES), F32),
+            vm((seq, LANES), BF16),
+            vm((seq, LANES), F32),
+            vm((seq, LANES), BF16),
+            vm((seq, LANES), BF16),
+            vm((seq, LANES), BF16),
+            vm((seq, LANES), F32),
+            vm((seq, LANES), F32),
+            vm((seq // BLOCK, STATE, LANES), F32),
+            vm((seq // BLOCK, STATE, LANES), F32),
+            vm((seq, LANES), BF16),
+            vm((q * BLOCK, n * LANES), BF16),
+            vm((q, BLOCK, q * LANES), BF16),
+            dma((q,)), dma((q,)), dma((q, q)), dma((q, q)), dma((q, q)), dma((q, q)),
+            dma((q, 2)), dma((q, 2)), dma((q + 1, q)), dma((q + 1, q)),
+            dma((n, 2)), dma((n, 2)), dma((n,)), dma((n,)), dma((q,)), dma((q,)),
+            dma((q,)), dma((q,)), dma((q, q)), dma((q, q)), dma((q,)), dma((q,)),
+            dma((q,)), dma((q,)), dma((10,)),
+        ],
+        compiler_params=pltpu.CompilerParams(
+            collective_id=0, has_side_effects=True, vmem_limit_bytes=56 << 20
+        ),
+        name="whole",
+    )(nrm, wv, wg, wk, wr, ws, wo, taps, offsets, rates, gain)
+
+
+def own_lanes(fwd, bwd, n):
+    both = jnp.stack([fwd.reshape(fwd.shape[0], n, -1), bwd.reshape(bwd.shape[0], n, -1)], 2)
+    both = both.reshape(fwd.shape[0], n, -1)
+    both = jnp.pad(both, ((0, 0), (0, 0), (0, LANES - both.shape[2])))
+    return both.transpose(1, 0, 2)
+
+
+def headwise(
+    n,
+    q,
+    tokens,
+    in_gain,
+    w_value,
+    w_gate,
+    w_in_key,
+    w_read,
+    w_step_fwd,
+    w_step_bwd,
+    conv_value,
+    conv_key,
+    conv_read,
+    step_bias,
+    rate,
+    norm_gain,
+    w_out,
+):
+    s = lax.axis_index("sp")
+    group = s // q
+    nrm = normalize(tokens.astype(F32), in_gain.astype(F32)).astype(BF16)
+    steps = own_lanes(w_step_fwd, w_step_bwd, n)[:, :, :16].transpose(0, 2, 1)
+
+    def cut(x, j):
+        return lax.dynamic_slice_in_dim(x, j * LANES, LANES, 1)
+
+    taps = jnp.concatenate([cut(conv_value, s), cut(conv_key, group), cut(conv_read, group)], 1)
+    small = own_lanes(
+        jnp.stack([step_bias[0], rate[0]]), jnp.stack([step_bias[1], rate[1]]), n
+    )
+    small = lax.dynamic_index_in_dim(small, s, 0, keepdims=False)
+    gain = lax.dynamic_slice_in_dim(norm_gain, s * LANES, LANES, 0).astype(F32)[None]
+    halves = whole(
+        n, q, nrm, w_value, w_gate, w_in_key, w_read, steps, w_out,
+        taps.astype(F32), small[0:1], small[1:2], gain,
+    )
+    total = (halves[0].astype(F32) + halves[1].astype(F32)).astype(BF16)
+    return total.reshape(q, BLOCK, q, LANES).transpose(1, 2, 0, 3).reshape(BLOCK, n * LANES)
+
+
+def whole_heads(mesh):
+    n, q = mesh.shape["sp"], math.isqrt(mesh.shape["sp"])
+
+    def run(*args):
+        cols, keys = args[2].shape[1], args[4].shape[1]
+        ready = (
+            q * q == n
+            and mesh.shape["tp"] == 2
+            and cols == n * LANES
+            and args[14].shape[1] == LANES
+            and keys == q * LANES
+            and q % 2 == 0
+            and args[0].shape[1] == n * LANES
+            and args[0].shape[0] == BLOCK
+        )
+        return headwise(n, q, *args) if ready else body(*args)
+
+    return run
+
+
 def solution(mesh):
     in_specs = (
         P("sp", None),
@@ -223,4 +637,4 @@
         P("tp", "sp"),
     )
     out_specs = P("sp", None)
-    return jax.shard_map(body, mesh=mesh, in_specs=in_specs, out_specs=out_specs, check_vma=False)
+    return jax.shard_map(whole_heads(mesh), mesh=mesh, in_specs=in_specs, out_specs=out_specs, check_vma=False)

time: 917 us -> 168 us (0.18)
  waiting for transfers between devices: 670 us -> 0 us
  Pallas kernels: 0 us -> 157 us
  blocking collectives: 81.3 us -> 0 us
  other arithmetic: 57.3 us -> 5.52 us
  matrix products: 40.6 us -> 0 us
  local copies, waits for them, and re-layouts: 42.6 us -> 4.66 us
  between operations: 14.6 us -> 0.13 us
    all_gather x7 -> x0, waiting for transfers between devices: 654 us -> none  [the longest x2 319 us: entering_2(): everything = jax.tree.map(lambda part: lax.all_gather(part, axis), x)]
    pallas_call x0 -> x1, Pallas kernels: none -> 157 us  [whole(): pl.pallas_call(functools.partial(whole_kernel, n, q), out_shape=jax.Shape...]
    all_gather x3 -> x0, blocking collectives: 50 us -> none  [the longest x1 24.5 us: body(): lax.all_gather(w_step_fwd, 'sp', axis=0, tiled=True)]
    select_n x32 -> x0, other arithmetic: 46.9 us -> none  [step(): return jax.tree.map(lambda a, b: jnp.where(reached, a, b), new, before)]
    dot_general x15 -> x0, matrix products: 40.6 us -> none  [the longest x6 15.6 us: body(): jnp.dot(normed, weight, preferred_element_type=jnp.float32)]
    unnamed x1 -> x0, blocking collectives: 31.4 us -> none
    mul x35 -> x0, local copies, waits for them, and re-layouts: 23.7 us -> none  [the longest x32 21.9 us: chain(): after_pair[0][:, None, None] * before_pair[1] + after_pair[1]]
    reduce_scatter x1 -> x0, waiting for transfers between devices: 9.54 us -> none  [body(): lax.psum_scatter(jnp.dot(normed_heads, out_whole, preferred_element_type=...]
  transfers between devices with their start and end apart: 10 -> 0, of which waited for: 9 -> 0; matrix products, arithmetic and copies ran while one was open for 14% -> 0% of each run, Pallas kernels for 0% -> 0%
where the time goes in v2:
time: 168 us
  Pallas kernels  157 us (93%)
  other arithmetic  5.52 us (3%)
  local copies, waits for them, and re-layouts  4.66 us (3%)
    pallas_call x1, Pallas kernels, whole(): pl.pallas_call(functools.partial(whole_kernel, n, q), out_shape=jax.Shape...  157 us

profile of v2, /device:TPU:19, one launch (start us, length us, event | category | flops | bytes accessed | tf_op | source)
XLA Modules:
  0.0 167.5 jit_solution(10574672190328059913)
XLA Ops:
  0.0 0.0 copy-start
  0.0 1.3 bitcast_convert_fusion.gain
  1.3 0.0 copy-start.3
  1.3 1.3 fusion
  2.6 0.0 copy-done.5
  2.6 0.0 copy-done
  2.7 0.8 constant_dynamic-slice_fusion
  3.4 0.6 maximum_convert_fusion.taps
  4.0 0.1 stack_reshape.14
  4.1 0.1 copy.26
  4.2 0.1 stack_reshape.15
  4.3 0.1 copy.27
  4.4 0.2 dynamic-slice_reduce_fusion
  4.6 0.6 slice_bitcast_fusion.1
  5.2 0.0 copy-done.2
  5.2 0.1 pad_bitcast_fusion
  5.3 0.6 slice_bitcast_fusion.ws
  6.0 0.0 copy-done.1
  6.0 1.0 fusion.2.nrm
  7.0 157.2 %whole.1 = bf16[2,4,128,512]{3,2,1,0:T(8,128)(2,1)} custom-call(bf16[128,2048]{1,0:T(8,128)(2,1)} %fusion.2.nrm, bf16[128,2048]{1,0:T(8,128)(2,1)} %wv.1, bf16[128,2048]{1,0:T(8,128)(2,1)} %wg.1, bf16[128,512]{1,0:T(8,128)(2,1)} %wk.1, bf16[128,512]{1,0:T(8,128)(2,1)} %wr.1, bf16[16,16,128]{2,1,0:T(8,128)(2,1)} %slice_bitcast_fusion.ws, ...), custom_call_target="tpu_custom_call" | custom-call | tf_op jit(solution)/shard_map/whole/pallas_call | solution.py:517
  164.2 1.3 add_convert_fusion
  165.5 0.1 convert_element_type.41
  165.7 0.7 copy.28
  166.3 1.2 reshape.30
  (16 shorter events, 0.1 us)
Async XLA Ops:
  0.0 2.7 %copy-start = (bf16[5,2048]{1,0:T(8,128)(2,1)S(1)}, bf16[5,2048]{1,0:T(8,128)(2,1)}, u32[]{:S(2)}) copy-start(bf16[5,2048]{1,0:T(8,128)(2,1)} %param.23) | copy-start | bytes 61444
  1.3 1.3 copy-start.5
  1.3 1.3 copy-start.6
  1.3 2.8 %copy-start.4 = (bf16[2048]{0:T(1024)(128)(2,1)S(1)}, bf16[2048]{0:T(1024)(128)(2,1)}, u32[]{:S(2)}) copy-start(bf16[2048]{0:T(1024)(128)(2,1)} %param.16) | copy-start | bytes 12292
  1.3 3.9 %copy-start.2 = (bf16[128,32]{0,1:T(8,128)(2,1)S(1)}, bf16[128,32]{0,1:T(8,128)(2,1)}, u32[]{:S(2)}) copy-start(bf16[128,32]{0,1:T(8,128)(2,1)} %param.22) | copy-start | bytes 24580
  1.3 3.9 %copy-start.3 = (bf16[128,32]{0,1:T(8,128)(2,1)S(1)}, bf16[128,32]{0,1:T(8,128)(2,1)}, u32[]{:S(2)}) copy-start(bf16[128,32]{0,1:T(8,128)(2,1)} %param.21) | copy-start | bytes 24580
  2.6 3.4 %copy-start.1 = (bf16[128,2048]{1,0:T(8,128)(2,1)S(1)}, bf16[128,2048]{1,0:T(8,128)(2,1)}, u32[]{:S(2)}) copy-start(bf16[128,2048]{1,0:T(8,128)(2,1)} %param.15) | copy-start | bytes 1572868

commit v3 on v2

--- a/solution.py
+++ b/solution.py
@@ -242,8 +242,8 @@
 
 
 def whole_kernel(
-    n, q, nrm, wv, wg, wk, wr, ws, wo, taps, offsets, rates, gain, both,
-    tok, wts, wst, wout, raw, gate, pre, vals, keys, reads, cums, yy, injf, injb, nh, full, part,
+    n, q, nrm, wv, wg, wk, wr, ws, wo, taps, offsets, rates, gain, out,
+    tok, wts, wst, wout, raw, gate, pre, vals, keys, reads, cums, yy, injf, injb, carf, carb, nh, full, part, both,
     tzs, tzr, tps, tpr, tss, tsr, kzs, kzr, kps, kpr, vs, vr, ss, sr, os, orr,
     as_, ar, bs, br, es, er, fs, fr, ls,
 ):
@@ -371,7 +371,7 @@
                 swaps[dz, dp].wait_recv()
         project(lax.rem(z + q - dz, q))
 
-    @pl.loop(0, blocks)
+    @pl.loop(0, blocks, unroll=2)
     def _(i):
         r0 = pl.multiple_of(i * BLOCK, BLOCK)
         for b, dst in enumerate((vals, keys, reads)):
@@ -391,7 +391,7 @@
     lower = jnp.where(low, 1.0, 0.0).astype(F32)
     upper = jnp.where(ri <= ci, 1.0, 0.0).astype(F32)
 
-    @pl.loop(0, blocks)
+    @pl.loop(0, blocks, unroll=4)
     def _(i):
         r0 = pl.multiple_of(i * BLOCK, BLOCK)
         here = pl.ds(r0, BLOCK)
@@ -425,7 +425,7 @@
             scaled = (val32 * w).astype(BF16)
             dst[i] = jnp.dot(key_t, scaled, preferred_element_type=F32)
 
-    def carry(i, state, d, inj):
+    def carry(i, state, d, inj, kept):
         r0 = pl.multiple_of(i * BLOCK, BLOCK)
         here = pl.ds(r0, BLOCK)
         ec = jnp.exp(cums[here, :])
@@ -436,23 +436,23 @@
         add = jnp.dot(read, high, preferred_element_type=F32) + jnp.dot(
             read, rest, preferred_element_type=F32
         )
-        yy[here, :] = yy[here, :] + add * grown
+        kept[here, :] = add * grown
         end = grown[BLOCK - 1 : BLOCK, :] if d == 0 else grown[0:1, :]
         return state * end + inj[i]
 
     def advance(i, states):
         return (
-            carry(i, states[0], 0, injf),
-            carry(blocks - 1 - i, states[1], 1, injb),
+            carry(i, states[0], 0, injf, carf),
+            carry(blocks - 1 - i, states[1], 1, injb, carb),
         )
 
     zero = jnp.zeros((STATE, LANES), F32)
-    lax.fori_loop(0, blocks, advance, (zero, zero))
+    lax.fori_loop(0, blocks, advance, (zero, zero), unroll=4)
 
     def finish(i):
         r0 = pl.multiple_of(i * BLOCK, BLOCK)
         here = pl.ds(r0, BLOCK)
-        g = yy[here, :] * silu(gate[here, :].astype(F32))
+        g = (yy[here, :] + carf[here, :] + carb[here, :]) * silu(gate[here, :].astype(F32))
         sq = g * g
         m0 = jnp.sum(jnp.where(left, sq, 0.0), -1, keepdims=True) / HEAD_DIM
         m1 = jnp.sum(jnp.where(left, 0.0, sq), -1, keepdims=True) / HEAD_DIM
@@ -463,7 +463,7 @@
     for dz in range(1, q + 1):
         to = lax.rem(z + dz, q)
 
-        @pl.loop(0, q)
+        @pl.loop(0, q, unroll=4)
         def _(i):
             finish(to * q + i)
 
@@ -501,6 +501,11 @@
     keep.wait()
     for copy in across:
         copy.wait()
+    for a in range(q):
+        for b in range(q):
+            here = slice(a * LANES, (a + 1) * LANES)
+            total = both[0, b, :, here].astype(F32) + both[1, b, :, here].astype(F32)
+            out[:, (a * q + b) * LANES : (a * q + b + 1) * LANES] = total.astype(BF16)
     flat = [copy for pair in keyz for copy in pair]
     for copy in first + flat + list(plane.values()) + keyp + weights + list(swaps.values()):
         copy.wait_send()
@@ -516,7 +521,7 @@
     seq = n * depth
     return pl.pallas_call(
         functools.partial(whole_kernel, n, q),
-        out_shape=jax.ShapeDtypeStruct((2, q, BLOCK, q * LANES), BF16),
+        out_shape=jax.ShapeDtypeStruct((BLOCK, n * LANES), BF16),
         in_specs=[VMEM_SPEC] * 11,
         out_specs=VMEM_SPEC,
         scratch_shapes=[
@@ -534,9 +539,12 @@
             vm((seq, LANES), F32),
             vm((seq // BLOCK, STATE, LANES), F32),
             vm((seq // BLOCK, STATE, LANES), F32),
+            vm((seq, LANES), F32),
+            vm((seq, LANES), F32),
             vm((seq, LANES), BF16),
             vm((q * BLOCK, n * LANES), BF16),
             vm((q, BLOCK, q * LANES), BF16),
+            vm((2, q, BLOCK, q * LANES), BF16),
             dma((q,)), dma((q,)), dma((q, q)), dma((q, q)), dma((q, q)), dma((q, q)),
             dma((q, 2)), dma((q, 2)), dma((q + 1, q)), dma((q + 1, q)),
             dma((n, 2)), dma((n, 2)), dma((n,)), dma((n,)), dma((q,)), dma((q,)),
@@ -590,12 +598,10 @@
     )
     small = lax.dynamic_index_in_dim(small, s, 0, keepdims=False)
     gain = lax.dynamic_slice_in_dim(norm_gain, s * LANES, LANES, 0).astype(F32)[None]
-    halves = whole(
+    return whole(
         n, q, nrm, w_value, w_gate, w_in_key, w_read, steps, w_out,
         taps.astype(F32), small[0:1], small[1:2], gain,
     )
-    total = (halves[0].astype(F32) + halves[1].astype(F32)).astype(BF16)
-    return total.reshape(q, BLOCK, q, LANES).transpose(1, 2, 0, 3).reshape(BLOCK, n * LANES)
 
 
 def whole_heads(mesh):

time: 168 us -> 163 us (0.970)
  Pallas kernels: 157 us -> 154 us
    pallas_call x1, Pallas kernels: 157 us -> 154 us  [whole(): pl.pallas_call(functools.partial(whole_kernel, n, q), out_shape=jax.Shape...]
    unnamed x14 -> x15, local copies, waits for them, and re-layouts: 0.03 us -> 1.91 us
where the time goes in v3:
time: 163 us
  Pallas kernels  154 us (94%)
  local copies, waits for them, and re-layouts  4.52 us (3%)
  other arithmetic  4.26 us (3%)
    pallas_call x1, Pallas kernels, whole(): pl.pallas_call(functools.partial(whole_kernel, n, q), out_shape=jax.Shape...  154 us

profile of v3, /device:TPU:19, one launch (start us, length us, event | category | flops | bytes accessed | tf_op | source)
XLA Modules:
  0.0 162.7 jit_solution(2767502919288905482)
XLA Ops:
  0.0 0.0 copy-start
  0.0 1.3 bitcast_convert_fusion.gain
  1.3 0.0 copy-start.3
  1.4 1.3 fusion
  2.7 0.0 copy-done.5
  2.7 0.0 copy-done.6
  2.7 0.0 copy-done
  2.8 0.8 constant_dynamic-slice_fusion
  3.5 0.6 maximum_convert_fusion.taps
  4.1 0.0 copy-done.4
  4.1 0.1 stack_reshape.14
  4.2 0.1 copy.24
  4.3 0.1 stack_reshape.15
  4.4 0.1 copy.25
  4.5 0.2 dynamic-slice_reduce_fusion
  4.7 0.6 slice_bitcast_fusion.1
  5.2 0.0 copy-done.2
  5.2 0.0 copy-done.3
  5.3 0.1 pad_bitcast_fusion
  5.4 0.6 slice_bitcast_fusion.ws
  6.0 0.0 copy-done.1
  6.0 1.0 fusion.2.nrm
  7.0 153.8 %whole.1 = bf16[128,2048]{1,0:T(8,128)(2,1)} custom-call(bf16[128,2048]{1,0:T(8,128)(2,1)} %fusion.2.nrm, bf16[128,2048]{1,0:T(8,128)(2,1)} %wv.1, bf16[128,2048]{1,0:T(8,128)(2,1)} %wg.1, bf16[128,512]{1,0:T(8,128)(2,1)} %wk.1, bf16[128,512]{1,0:T(8,128)(2,1)} %wr.1, bf16[16,16,128]{2,1,0:T(8,128)(2,1)} %slice_bitcast_fusion.ws, bf16[2048,128]{1,0:T(8,128)(2,1)} %wo.1, ...), custom_call_target="tpu_custom_call" | custom-call | tf_op jit(solution)/shard_map/whole/pallas_call | solution.py:522
  160.8 1.9 %copy.27 = bf16[128,2048]{1,0:T(8,128)(2,1)} copy(bf16[128,2048]{1,0:T(8,128)(2,1)} %whole.1) | data formatting | bytes 1048576
  (13 shorter events, 0.1 us)
Async XLA Ops:
  0.0 2.7 %copy-start = (bf16[5,2048]{1,0:T(8,128)(2,1)S(1)}, bf16[5,2048]{1,0:T(8,128)(2,1)}, u32[]{:S(2)}) copy-start(bf16[5,2048]{1,0:T(8,128)(2,1)} %param.23) | copy-start | bytes 61444
  1.3 1.3 copy-start.5
  1.3 1.3 copy-start.6
  1.3 2.8 %copy-start.4 = (bf16[2048]{0:T(1024)(128)(2,1)S(1)}, bf16[2048]{0:T(1024)(128)(2,1)}, u32[]{:S(2)}) copy-start(bf16[2048]{0:T(1024)(128)(2,1)} %param.16) | copy-start | bytes 12292
  1.3 3.9 %copy-start.2 = (bf16[128,32]{0,1:T(8,128)(2,1)S(1)}, bf16[128,32]{0,1:T(8,128)(2,1)}, u32[]{:S(2)}) copy-start(bf16[128,32]{0,1:T(8,128)(2,1)} %param.22) | copy-start | bytes 24580
  1.3 3.9 %copy-start.3 = (bf16[128,32]{0,1:T(8,128)(2,1)S(1)}, bf16[128,32]{0,1:T(8,128)(2,1)}, u32[]{:S(2)}) copy-start(bf16[128,32]{0,1:T(8,128)(2,1)} %param.21) | copy-start | bytes 24580
  2.6 3.4 %copy-start.1 = (bf16[128,2048]{1,0:T(8,128)(2,1)S(1)}, bf16[128,2048]{1,0:T(8,128)(2,1)}, u32[]{:S(2)}) copy-start(bf16[128,2048]{1,0:T(8,128)(2,1)} %param.15) | copy-start | bytes 1572868

commit v4 on v3

--- a/solution.py
+++ b/solution.py
@@ -260,8 +260,15 @@
     def span(i, size):
         return pl.ds(pl.multiple_of(i * size, size), size)
 
+    px = p + 1 - 2 * lax.rem(p, 2)
+    py = lax.rem(p + 2, q)
+    pd = lax.rem(px + 2, q)
+    side = {"x": (z * q + px, t), "y": (z * q + py, t)}
+
+    def chip(dz, where):
+        return lax.rem(z + q - dz, q) * q + where
+
     greet([(lax.rem(s + k, n), t) for k in range(1, n)] + [sibling])
-    done, sent = [], []
 
     def local(src, dst, i):
         copy = pltpu.make_async_copy(src, dst, ls.at[i])
@@ -283,8 +290,8 @@
             ]
         )
     plane, keyp = {}, []
-    for dp in range(1, q):
-        plane[0, dp] = push(nrm.at[rows], tok.at[s, t], tps.at[0, dp], tpr.at[0, dp], (at(0, dp), t))
+    for i, to in enumerate("xy"):
+        plane[0, to] = push(nrm.at[rows], tok.at[s, t], tps.at[0, i], tpr.at[0, i], side[to])
     for dp in range(1, q):
         for i, (w, col) in enumerate(((wk, kcol), (wr, rcol))):
             keyp.append(
@@ -315,15 +322,15 @@
         )
     swaps = {}
 
-    def swap(dz, dp):
-        src = at(q - dz, q - dp)
-        swaps[dz, dp] = push(tok.at[src, t], tok.at[src, t], tss.at[dz, dp], tsr.at[dz, dp], sibling)
+    def swap(dz, i):
+        src = chip(dz, (p, px, py, pd)[i])
+        swaps[dz, i] = push(tok.at[src, t], tok.at[src, t], tss.at[dz, i], tsr.at[dz, i], sibling)
 
     for dz in range(1, q):
         src = at(q - dz, 0)
         first[dz - 1].wait_recv()
-        for dp in range(1, q):
-            plane[dz, dp] = push(tok.at[src, t], tok.at[src, t], tps.at[dz, dp], tpr.at[dz, dp], (at(0, dp), t))
+        for i, to in enumerate("xy"):
+            plane[dz, to] = push(tok.at[src, t], tok.at[src, t], tps.at[dz, i], tpr.at[dz, i], side[to])
         swap(dz, 0)
         for copy in keyz[dz - 1]:
             copy.wait_recv()
@@ -342,16 +349,14 @@
     raw[seq + 8 : seq + 16, :] = jnp.zeros((8, wide), F32)
     for copy in locals_:
         copy.wait()
-    for copy in weights + keyp:
-        copy.wait_recv()
 
     def project(plane_index):
         @pl.loop(0, q // 2)
         def _(i):
-            chip = plane_index * q + 2 * i
-            r0 = pl.multiple_of(chip * BLOCK, 2 * BLOCK)
+            pair = plane_index * q + 2 * i
+            r0 = pl.multiple_of(pair * BLOCK, 2 * BLOCK)
             at2 = pl.ds(r0, 2 * BLOCK)
-            x = tok[pl.ds(chip, 2)].reshape(2 * BLOCK, tok.shape[3])
+            x = tok[pl.ds(pair, 2)].reshape(2 * BLOCK, tok.shape[3])
             got = jnp.dot(x, wts[...], preferred_element_type=F32).astype(BF16)
             for i_, b_ in ((0, 0), (2, 1), (3, 2)):
                 raw[pl.ds(r0 + 8, 2 * BLOCK), b_ * LANES : (b_ + 1) * LANES] = got[
@@ -362,14 +367,32 @@
             u = u.astype(BF16).astype(F32) + offsets[...]
             pre[at2, :] = jnp.maximum(u, 0.0) + jnp.log1p(jnp.exp(-jnp.abs(u)))
 
+    quarter = half // 2
+
+    def relay(dz):
+        for i, (near_by, other) in enumerate((("x", "y"), ("y", "x"))):
+            plane[dz, near_by].wait_recv()
+            got = tok.at[chip(dz, (px, py)[i]), t, pl.ds(i * quarter, quarter)]
+            plane[dz, other + "d"] = push(got, got, tps.at[dz, 2 + i], tpr.at[dz, 2 + i], side[other])
+            swap(dz, 1 + i)
+
+    def use(dz):
+        plane[dz, "yd"].wait_recv()
+        plane[dz, "xd"].wait_recv()
+        swap(dz, 3)
+        for i in range(q):
+            if (dz, i) != (0, 0):
+                swaps[dz, i].wait_recv()
+        project(lax.rem(z + q - dz, q))
+
     for dz in range(q):
-        for dp in range(1, q):
-            plane[dz, dp].wait_recv()
-            swap(dz, dp)
-        for dp in range(q):
-            if (dz, dp) != (0, 0):
-                swaps[dz, dp].wait_recv()
-        project(lax.rem(z + q - dz, q))
+        relay(dz)
+        if dz == 1:
+            for copy in weights + keyp:
+                copy.wait_recv()
+        if dz >= 1:
+            use(dz - 1)
+    use(q - 1)
 
     @pl.loop(0, blocks, unroll=2)
     def _(i):
@@ -413,8 +436,8 @@
             gap = jnp.where(low, c[:, h : h + 1] - ct[h : h + 1, :], c[:, h + 2 : h + 3] - ct[h + 2 : h + 3, :])
             sb = stt[h + 2 : h + 3, :]
             e = jnp.exp(gap) * jnp.where(low, stt[h : h + 1, :], sb) + jnp.where(diag, sb, 0.0)
-            side = left if h == 0 else jnp.logical_not(left)
-            own = jnp.where(side, val32, 0.0).astype(BF16)
+            mask = left if h == 0 else jnp.logical_not(left)
+            own = jnp.where(mask, val32, 0.0).astype(BF16)
             total = total + jnp.dot((score * e).astype(BF16), own, preferred_element_type=F32)
         yy[here, :] = total
         c_end = jnp.where(fwd[0:1], c[BLOCK - 1 : BLOCK, :], c[0:1, :])
@@ -473,17 +496,23 @@
             )
     near = {}
     keep = local(nh.at[span(z, q * BLOCK)], full.at[:, mine], 8)
-    for dp in range(1, q):
-        near[0, dp] = push(
-            nh.at[span(z, q * BLOCK)], full.at[:, mine], bs.at[0, dp], br.at[0, dp], (at(0, dp), t)
+    for i, to in enumerate("xy"):
+        near[0, to] = push(
+            nh.at[span(z, q * BLOCK)], full.at[:, mine], bs.at[0, i], br.at[0, i], side[to]
         )
     for dz in range(1, q):
         away[dz - 1].wait_recv()
         got = full.at[:, span(at(q - dz, 0), LANES)]
-        for dp in range(1, q):
-            near[dz, dp] = push(got, got, bs.at[dz, dp], br.at[dz, dp], (at(0, dp), t))
+        for i, to in enumerate("xy"):
+            near[dz, to] = push(got, got, bs.at[dz, i], br.at[dz, i], side[to])
+    rest_rows = q * BLOCK // 2
+    for dz in range(q):
+        for i, (near_by, other) in enumerate((("x", "y"), ("y", "x"))):
+            near[dz, near_by].wait_recv()
+            got = full.at[pl.ds(i * rest_rows, rest_rows), span(chip(dz, (px, py)[i]), LANES)]
+            near[dz, other + "d"] = push(got, got, bs.at[dz, 2 + i], br.at[dz, 2 + i], side[other])
     keep.wait()
-    for copy in outs + list(near.values()):
+    for copy in outs + [near[dz, to] for dz in range(q) for to in ("xd", "yd")]:
         copy.wait_recv()
     legs = []
     for dp in range(1, q + 1):
@@ -615,7 +644,7 @@
             and cols == n * LANES
             and args[14].shape[1] == LANES
             and keys == q * LANES
-            and q % 2 == 0
+            and q == 4
             and args[0].shape[1] == n * LANES
             and args[0].shape[0] == BLOCK
         )

time: 163 us -> 159 us (0.975)
  Pallas kernels: 154 us -> 150 us
    pallas_call x1, Pallas kernels: 154 us -> 150 us  [whole(): pl.pallas_call(functools.partial(whole_kernel, n, q), out_shape=jax.Shape...]
where the time goes in v4:
time: 159 us
  Pallas kernels  150 us (94%)
  local copies, waits for them, and re-layouts  4.52 us (3%)
  other arithmetic  4.26 us (3%)
    pallas_call x1, Pallas kernels, whole(): pl.pallas_call(functools.partial(whole_kernel, n, q), out_shape=jax.Shape...  150 us

profile of v4, /device:TPU:19, one launch (start us, length us, event | category | flops | bytes accessed | tf_op | source)
XLA Modules:
  0.0 158.7 jit_solution(13786994611912047185)
XLA Ops:
  0.0 0.0 copy-start
  0.0 1.3 bitcast_convert_fusion.gain
  1.3 0.0 copy-start.3
  1.4 1.3 fusion
  2.7 0.0 copy-done.5
  2.7 0.0 copy-done.6
  2.7 0.0 copy-done
  2.8 0.8 constant_dynamic-slice_fusion
  3.5 0.6 maximum_convert_fusion.taps
  4.1 0.0 copy-done.4
  4.1 0.1 stack_reshape.14
  4.2 0.1 copy.24
  4.3 0.1 stack_reshape.15
  4.4 0.1 copy.25
  4.5 0.2 dynamic-slice_reduce_fusion
  4.7 0.6 slice_bitcast_fusion.1
  5.2 0.0 copy-done.2
  5.2 0.0 copy-done.3
  5.3 0.1 pad_bitcast_fusion
  5.4 0.6 slice_bitcast_fusion.ws
  6.0 0.0 copy-done.1
  6.0 1.0 fusion.2.nrm
  7.0 149.8 %whole.1 = bf16[128,2048]{1,0:T(8,128)(2,1)} custom-call(bf16[128,2048]{1,0:T(8,128)(2,1)} %fusion.2.nrm, bf16[128,2048]{1,0:T(8,128)(2,1)} %wv.1, bf16[128,2048]{1,0:T(8,128)(2,1)} %wg.1, bf16[128,512]{1,0:T(8,128)(2,1)} %wk.1, bf16[128,512]{1,0:T(8,128)(2,1)} %wr.1, bf16[16,16,128]{2,1,0:T(8,128)(2,1)} %slice_bitcast_fusion.ws, bf16[2048,128]{1,0:T(8,128)(2,1)} %wo.1, ...), custom_call_target="tpu_custom_call" | custom-call | tf_op jit(solution)/shard_map/whole/pallas_call | solution.py:551
  156.9 1.9 %copy.27 = bf16[128,2048]{1,0:T(8,128)(2,1)} copy(bf16[128,2048]{1,0:T(8,128)(2,1)} %whole.1) | data formatting | bytes 1048576
  (13 shorter events, 0.1 us)
Async XLA Ops:
  0.0 2.7 %copy-start = (bf16[5,2048]{1,0:T(8,128)(2,1)S(1)}, bf16[5,2048]{1,0:T(8,128)(2,1)}, u32[]{:S(2)}) copy-start(bf16[5,2048]{1,0:T(8,128)(2,1)} %param.23) | copy-start | bytes 61444
  1.3 1.3 copy-start.5
  1.3 1.3 copy-start.6
  1.3 2.8 %copy-start.4 = (bf16[2048]{0:T(1024)(128)(2,1)S(1)}, bf16[2048]{0:T(1024)(128)(2,1)}, u32[]{:S(2)}) copy-start(bf16[2048]{0:T(1024)(128)(2,1)} %param.16) | copy-start | bytes 12292
  1.3 3.9 %copy-start.2 = (bf16[128,32]{0,1:T(8,128)(2,1)S(1)}, bf16[128,32]{0,1:T(8,128)(2,1)}, u32[]{:S(2)}) copy-start(bf16[128,32]{0,1:T(8,128)(2,1)} %param.22) | copy-start | bytes 24580
  1.3 3.9 %copy-start.3 = (bf16[128,32]{0,1:T(8,128)(2,1)S(1)}, bf16[128,32]{0,1:T(8,128)(2,1)}, u32[]{:S(2)}) copy-start(bf16[128,32]{0,1:T(8,128)(2,1)} %param.21) | copy-start | bytes 24580
  2.6 3.4 %copy-start.1 = (bf16[128,2048]{1,0:T(8,128)(2,1)S(1)}, bf16[128,2048]{1,0:T(8,128)(2,1)}, u32[]{:S(2)}) copy-start(bf16[128,2048]{1,0:T(8,128)(2,1)} %param.15) | copy-start | bytes 1572868
